TPU v7x, 512 devices: a whole 4x4x16 slice. The times are simulated.
512 devices in a mesh: fs: 128 (over z, x, core), tp: 4 (over y).
Axes of the slice: x: 4, y: 4, z: 16, core: 2. Of those that a mesh axis runs over, the one named last changes fastest.
Arguments:
- normed_input: bfloat16 [81920, 2048], P('fs'), may hold values from -448 to 448
- key_cotangent: bfloat16 [81920, 512], P('fs', 'tp'), may hold values from -0.01953125 to 0.01953125
- value_cotangent: bfloat16 [81920, 1024], P('fs', 'tp'), may hold values from -0.01953125 to 0.01953125
- key_factor: bfloat16 [512, 128], P('tp'), may hold values from -2.8 to 2.8
- value_factor: bfloat16 [1024, 128], P('tp'), may hold values from -2.8 to 2.8
- key_weight: float32 [2048, 512], P('fs', 'tp'), may hold values from -0.125 to 0.125
- value_weight: float32 [2048, 1024], P('fs', 'tp'), may hold values from -0.125 to 0.125
- first_moments: float32 [2, 2048, 128], P(None, 'fs', 'tp'), may hold values from -0.6 to 0.6
- second_moments: float32 [2, 2048, 128], P(None, 'fs', 'tp'), may hold values from 0.001 to 0.1
Outputs:
- first_new: float32 [2, 2048, 128], P(None, 'fs', 'tp')
- second_new: float32 [2, 2048, 128], P(None, 'fs', 'tp')
- new_key_weight: float32 [2048, 512], P('fs', 'tp')
- new_value_weight: float32 [2048, 1024], P('fs', 'tp')
- key_copy: bfloat16 [2048, 512], P(None, 'tp')
- value_copy: bfloat16 [2048, 1024], P(None, 'tp')
All inputs are finite; a program needn't handle non-finite values.
Results may differ from a plain program's by a relative error of at most 0.005.
Values may be sent and summed in bfloat16 or wider, within the bound.
A program may use at most 64 MiB of HBM per device.

v0:
```python
import jax
import jax.numpy as jnp
from jax import lax
from jax.sharding import Mesh
from jax.sharding import PartitionSpec as P

D = 2048
RANK = 128
FS = ("fs_0", "fs_1", "fs_2")


step_rate = 0.05
clip_target = 0.1
beta_first = 0.8
beta_second = 0.95
small_eps = 1e-08
norm_eps = 1e-06


def in_blocks(value, dim, count):
    shape = value.shape
    pieces = value.reshape(*shape[:dim], count, shape[dim] // count, *shape[dim + 1 :])
    return jnp.moveaxis(pieces, dim, 0)


def summed_on_arrival(value, axis, dim):
    count = lax.axis_size(axis)
    pieces = lax.all_to_all(in_blocks(value, dim, count), axis, 0, 0, tiled=True)
    return jnp.sum(pieces, axis=0)


def sum_by_axis(value, axes, dim):
    far, near = axes
    pieces = in_blocks(value, dim, lax.axis_size(far))
    nearer = summed_on_arrival(pieces, near, dim + 1)
    arrived = lax.all_to_all(nearer, far, split_axis=0, concat_axis=0, tiled=True)
    return arrived.sum(axis=0)


def from_everyone(value, axis):
    count = lax.axis_size(axis)
    return lax.all_to_all(
        jnp.broadcast_to(value[None], (count, *value.shape)), axis, 0, 0, tiled=True
    )


def of_everyone(value, axis):
    everything = from_everyone(value, axis)
    return jnp.sum(everything, axis=0)


def one_axis_at_a_time(value, axes):
    far, near = axes
    nearer = of_everyone(value, near)
    return of_everyone(nearer, far)


def laid_out(pieces, dim):
    shape = list(pieces.shape[1:])
    shape[dim] *= pieces.shape[0]
    return jnp.moveaxis(pieces, 0, dim).reshape(shape)


def gathered_copies(value, axis, dim):
    return laid_out(from_everyone(value, axis), dim)


def in_one_piece(arrays, axis, dim, along):
    ends, at = ([], 0)
    for a in arrays[:-1]:
        at += a.shape[along]
        ends.append(at)
    both = jnp.concatenate(arrays, axis=along)
    return tuple(jnp.split(lax.all_gather(both, axis, axis=dim, tiled=True), ends, axis=along))


def split_product(normed_input, reduced):
    upper = reduced.astype(jnp.bfloat16)
    lower = (reduced - upper.astype(jnp.float32)).astype(jnp.bfloat16)
    joined = jnp.concatenate([upper, lower], axis=1)
    width = reduced.shape[1]
    both = lax.dot_general(
        normed_input, joined, (((0,), (0,)), ((), ())), preferred_element_type=jnp.float32
    )
    return both[:, :width] + both[:, width:]


def local(
    normed_input,
    key_cotangent,
    value_cotangent,
    key_factor,
    value_factor,
    key_weight,
    value_weight,
    first_moments,
    second_moments,
):
    rank_total = key_factor.shape[1]
    rank_dev = first_moments.shape[2]
    tok_rows = normed_input.shape[0]
    highest = lax.Precision.HIGHEST
    group_count = lax.axis_size("tp")
    key_reduced = jnp.dot(key_cotangent, key_factor, preferred_element_type=jnp.float32)
    value_reduced = jnp.dot(value_cotangent, value_factor, preferred_element_type=jnp.float32)
    arranged = jnp.stack(
        [
            key_reduced.reshape(tok_rows, group_count, rank_dev),
            value_reduced.reshape(tok_rows, group_count, rank_dev),
        ],
        axis=2,
    )
    arranged = arranged.reshape(tok_rows, 2 * rank_total)
    own_reduced = summed_on_arrival(arranged, "tp", 1)
    own_terms = sum_by_axis(split_product(normed_input, own_reduced), (("fs_0", "fs_1"), "fs_2"), 0)
    own_key = own_terms[:, :rank_dev]
    own_value = own_terms[:, rank_dev:]
    proj_key, proj_value = (own_key, own_value)
    projected = jnp.stack([proj_key, proj_value])
    prior_first, prior_second = (first_moments, second_moments)
    total_sq = one_axis_at_a_time(
        jnp.sum(projected * projected), (("fs_0", "fs_1"), ("fs_2", "tp"))
    )
    clip_limit = clip_target * jnp.sqrt(jnp.float32(2 * D * RANK))
    clip_factor = jnp.minimum(1.0, clip_limit / jnp.sqrt(total_sq + norm_eps))
    scaled = clip_factor * projected
    first_new = beta_first * prior_first + (1.0 - beta_first) * scaled
    second_new = beta_second * prior_second + (1.0 - beta_second) * scaled * scaled
    direction = first_new / (jnp.sqrt(second_new) + small_eps)
    full_direction = gathered_copies(direction, "tp", 2)
    first_out, second_out = (first_new, second_new)
    back = (((1,), (1,)), ((), ()))
    update_key = lax.dot_general(
        full_direction[0], key_factor.astype(jnp.float32), back, precision=highest
    )
    update_value = lax.dot_general(
        full_direction[1], value_factor.astype(jnp.float32), back, precision=highest
    )
    new_key = key_weight - step_rate * update_key
    new_value = value_weight - step_rate * update_value
    key_copy, value_copy = in_one_piece(
        (new_key.astype(jnp.bfloat16), new_value.astype(jnp.bfloat16)), FS, 0, 1
    )
    return (first_out, second_out, new_key, new_value, key_copy, value_copy)


def solution(mesh):
    torus = Mesh(mesh.devices.reshape(16, 4, 2, mesh.shape["tp"]), ("fs_0", "fs_1", "fs_2", "tp"))
    return jax.shard_map(
        local,
        mesh=torus,
        in_specs=(
            P(FS, None),
            P(FS, "tp"),
            P(FS, "tp"),
            P("tp", None),
            P("tp", None),
            P(FS, "tp"),
            P(FS, "tp"),
            P(None, FS, "tp"),
            P(None, FS, "tp"),
        ),
        out_specs=(
            P(None, FS, "tp"),
            P(None, FS, "tp"),
            P(FS, "tp"),
            P(FS, "tp"),
            P(None, "tp"),
            P(None, "tp"),
        ),
        check_vma=False,
    )
```

profile of v0, /device:TPU:1, one launch (start us, length us, event | category | flops | bytes accessed | tf_op | source)
XLA Modules:
  0.0 269.5 jit_solution(1019508115857173768)
XLA Ops:
  7.2 0.0 copy-start
  7.2 0.0 all-gather.2.cloned.1.call-start
  7.2 1.3 fusion.11
  8.5 1.2 fusion.12
  9.8 0.1 pad_maximum_fusion
  9.8 12.4 %all_to_all.32 = f32[4,640,64]{1,2,0:T(8,128)S(1)} all-to-all(f32[4,640,64]{1,2,0:T(8,128)S(1)} %bitcast.29), channel_id=1, replica_groups=mesh['fs_0'=16,'fs_1'=4,'fs_2'=2,'tp'=4] {'tp'}, dimensions={0} | all-to-all | bytes 1310720 | tf_op jit(solution)/shard_map/all_to_all | solution.py:28
  22.3 0.0 copy-done
  22.3 0.6 convolution_bitcast_fusion
  22.9 0.1 slice_add_fusion
  23.0 1.3 copy.32
  24.3 2.3 copy.33
  26.6 1.7 reshape.24
  28.3 10.1 %all_to_all.33 = f32[2,1,65536]{2,1,0:T(1,128)} all-to-all(f32[2,1,65536]{2,1,0:T(1,128)S(1)} %reshape.24), channel_id=1, replica_groups=mesh['fs_0'=16,'fs_1'=4,'fs_2'=2,'tp'=4] {'fs_2'}, dimensions={0} | all-to-all | bytes 1048576 | tf_op jit(solution)/shard_map/all_to_all | solution.py:28
  38.4 0.5 broadcast.5
  38.9 3.2 %reduce.2 = f32[2,65536]{1,0:T(2,128)S(1)} reduce(f32[2,1,65536]{2,1,0:T(1,128)} %all_to_all.33, f32[]{:T(128)} %broadcast.5), dimensions={1}, to_apply=%all_to_all.21.reduce_sub_computation | reduce | bytes 1048580 | tf_op jit(solution)/shard_map/all_to_all | solution.py:28
  42.1 1.6 reshape.25
  43.7 0.0 copy-start.2
  43.8 1.4 reduce_sum.55
  45.2 0.3 reshape.26
  45.5 36.9 %all_to_all.34 = f32[64,1,1024]{2,1,0:T(1,128)S(1)} all-to-all(f32[64,1,1024]{2,1,0:T(1,128)S(1)} %reshape.26), channel_id=1, replica_groups=mesh['fs_0'=16,'fs_1'=4,'fs_2'=2,'tp'=4] {'fs_0','fs_1'}, dimensions={0} | all-to-all | bytes 524288 | tf_op jit(solution)/shard_map/all_to_all | solution.py:36
  82.4 1.3 reduce.3
  83.6 0.1 reshape.27
  83.8 0.1 reduce_sum.56
  83.9 0.1 slice_bitcast_fusion.1
  83.9 0.6 multiply_reduce_fusion
  84.6 0.6 broadcast_in_dim.6
  85.2 10.2 %all_to_all.35 = f32[8,1,1]{2,1,0:T(1,128)S(1)} all-to-all(f32[8,1,1]{2,1,0:T(1,128)S(1)} %broadcast_in_dim.6), channel_id=1, replica_groups=mesh['fs_0'=16,'fs_1'=4,'fs_2'=2,'tp'=4] {'fs_2','tp'}, dimensions={0} | all-to-all | bytes 64 | tf_op jit(solution)/shard_map/all_to_all | solution.py:42
  95.4 0.6 reduce_sum.58
  96.0 0.7 broadcast_in_dim.7
  96.6 18.0 %all_to_all.36 = f32[64,1,1]{2,1,0:T(1,128)S(1)} all-to-all(f32[64,1,1]{2,1,0:T(1,128)S(1)} %broadcast_in_dim.7), channel_id=1, replica_groups=mesh['fs_0'=16,'fs_1'=4,'fs_2'=2,'tp'=4] {'fs_0','fs_1'}, dimensions={0} | all-to-all | bytes 512 | tf_op jit(solution)/shard_map/all_to_all | solution.py:42
  114.6 0.7 reduce_sum.59
  116.0 0.0 copy-done.4
  116.0 0.0 copy-done.5
  116.0 0.6 add_divide_fusion
  116.6 0.1 reshape.28
  116.7 6.6 %all_to_all.37 = f32[4,1,1024]{2,1,0:T(1,128)S(1)} all-to-all(f32[4,1,1024]{2,1,0:T(1,128)S(1)} %reshape.28), channel_id=1, replica_groups=mesh['fs_0'=16,'fs_1'=4,'fs_2'=2,'tp'=4] {'tp'}, dimensions={0} | all-to-all | bytes 32768 | tf_op jit(solution)/shard_map/all_to_all | solution.py:42
  123.3 0.7 reduce.4
  124.0 0.1 reshape.29
  124.1 0.1 squeeze.7
  124.2 0.1 squeeze.6
  124.3 0.0 copy-done.1
  124.3 0.8 fusion.9
  125.1 1.5 fusion.10
  126.6 0.6 pad_maximum_fusion.2
  127.2 0.0 all-gather.2.cloned.1.call-update
  127.2 131.3 %all-gather.2.cloned.1.call-done = bf16[2048,384]{1,0:T(8,128)(2,1)} async-done(((bf16[16,384]{1,0:T(8,128)(2,1)}), bf16[2048,384]{1,0:T(8,128)(2,1)}) %all-gather.2.cloned.1.call-update) | async-done | bytes 1572880 | tf_op jit(solution)/shard_map/all_gather | solution.py:74
  258.5 1.9 split.8
  260.4 2.3 split.9
  (12 shorter events, 0.1 us)
Async XLA Ops:
  7.2 15.2 %copy-start = (bf16[640,2048]{1,0:T(8,128)(2,1)S(1)}, bf16[640,2048]{1,0:T(8,128)(2,1)}, u32[]{:S(2)}) copy-start(bf16[640,2048]{1,0:T(8,128)(2,1)} %param.9) | copy-start | bytes 7864324
  7.2 251.3 %all-gather.2.cloned.1.call-start = ((), (), s32[]{:S(2)}) async-start(), calls=%async_computation.6 | async-start | bytes 1585152 | tf_op jit(solution)/shard_map/all_gather | solution.py:74
  43.7 72.2 %copy-start.4 = (f32[2,16,32]{2,1,0:T(8,128)S(1)}, f32[2,16,32]{2,1,0:T(8,128)}, u32[]{:S(2)}) copy-start(f32[2,16,32]{2,1,0:T(8,128)} %param.17) | copy-start | bytes 12292
  43.7 72.2 %copy-start.5 = (f32[2,16,32]{2,1,0:T(8,128)S(1)}, f32[2,16,32]{2,1,0:T(8,128)}, u32[]{:S(2)}) copy-start(f32[2,16,32]{2,1,0:T(8,128)} %param.16) | copy-start | bytes 12292
  43.7 80.5 %copy-start.1 = (bf16[256,128]{1,0:T(8,128)(2,1)S(1)}, bf16[256,128]{1,0:T(8,128)(2,1)}, u32[]{:S(2)}) copy-start(bf16[256,128]{1,0:T(8,128)(2,1)} %param.13) | copy-start | bytes 196612
  43.7 80.5 %copy-start.3 = (f32[16,256]{1,0:T(8,128)S(1)}, f32[16,256]{1,0:T(8,128)}, u32[]{:S(2)}) copy-start(f32[16,256]{1,0:T(8,128)} %param.15) | copy-start | bytes 49156
  43.7 81.3 %copy-start.2 = (bf16[128,128]{1,0:T(8,128)(2,1)S(1)}, bf16[128,128]{1,0:T(8,128)(2,1)}, u32[]{:S(2)}) copy-start(bf16[128,128]{1,0:T(8,128)(2,1)} %param.12) | copy-start | bytes 98308
Sparse Core Ops, SparseCore 0:
  127.3 131.1 all-gather.1
where the time goes:
time: 270 us; the launch traced here: 269 us
  waiting for transfers between devices  131 us (49%)
  blocking collectives  94.1 us (35%)
  between operations  14.9 us (6%)
  local copies, waits for them, and re-layouts  13.8 us (5%)
  other arithmetic  9.92 us (4%)
  matrix products  5.38 us (2%)
    all_gather x1, waiting for transfers between devices, in_one_piece(): lax.all_gather(both, axis, axis=dim, tiled=True)  131 us
    all_to_all x1, blocking collectives, sum_by_axis(): lax.all_to_all(nearer, far, split_axis=0, concat_axis=0, tiled=True)  36.9 us
    all_to_all x3, blocking collectives, from_everyone(): lax.all_to_all(jnp.broadcast_to(value[None], (count, *value.shape)), axis...  34.7 us
    all_to_all x2, blocking collectives, summed_on_arrival(): lax.all_to_all(in_blocks(value, dim, count), axis, 0, 0, tiled=True)  22.5 us
  transfers between devices with their start and end apart: 1, of which 1 were waited for; matrix products, arithmetic and copies ran while one was open for 0% of the time, Pallas kernels for 0%

commit v1 on v0

v1 whole, which is shorter than its diff:
```python
import jax
import jax.numpy as jnp
from jax import lax
from jax.experimental import pallas as pl
from jax.experimental.pallas import tpu as pltpu
from jax.sharding import Mesh
from jax.sharding import PartitionSpec as P

D = 2048
RANK = 128
NZ, NX, NC, NY = 16, 4, 2, 4
FS = ("z", "x", "c")
TOK = 640
HALF = TOK // 2
NK = 128
NV = 256
NW = NK + NV

step_rate = 0.05
clip_target = 0.1
beta_first = 0.8
beta_second = 0.95
small_eps = 1e-08
norm_eps = 1e-06

NEAR = (1, 15, 14)
FAR = (4, 12, 8)
f32 = jnp.float32
bf16 = jnp.bfloat16


def kernel(
    x_hbm, ck_hbm, cv_hbm, fk_ref, fv_ref, kw_ref, vw_ref, m_ref, v_ref,
    first_ref, second_ref, nk_ref, nv_ref, ko_ref, vo_ref,
    x_vm, xt, ck, cv, wt, msend, yrecv, asend, crecv, xsend, xrecv, tsend, arecv, brecv, gy, mb, wb, sb,
    dirs, firsts, seconds, upd,
    in_sem, y_s, y_r, c_s, c_r, x_s, x_r, a_s, a_r, b_s, b_r, g_s, g_r, h_s, h_r,
    mf_s, mf_r, mn_s, mn_r, my_s, my_r, wf_s, wf_r, wn_s, wn_r, s_s, s_r,
    or_s, or_r, ol_s, ol_r, oc_s, oc_r,
):
    z, x, c, y = (lax.axis_index(n) for n in ("z", "x", "c", "y"))
    k, q = lax.div(z, 4), lax.rem(z, 4)
    other = 1 - c
    xc = x * 2 + c

    def zp(d):
        return lax.rem(z + d, NZ)

    def xp(d):
        return lax.rem(x + d, NX)

    def yp(d):
        return lax.rem(y + d, NY)

    def at_z(d):
        return (zp(d), x, c, y)

    def at_x(d):
        return (z, xp(d), c, y)

    def at_y(d):
        return (z, x, c, yp(d))

    partner = (z, x, other, y)

    def remote(src, dst, send, recv, to):
        return pltpu.make_async_remote_copy(
            src_ref=src, dst_ref=dst, send_sem=send, recv_sem=recv,
            device_id=to, device_id_type=pl.DeviceIdType.MESH,
        )

    loads = [
        pltpu.make_async_copy(ck_hbm, ck, in_sem.at[0]),
        pltpu.make_async_copy(cv_hbm, cv, in_sem.at[1]),
        pltpu.make_async_copy(x_hbm, x_vm, in_sem.at[2]),
    ]
    for load in loads:
        load.start()
    near_plane = [
        (z, xp(dx), c if dc == 0 else other, yp(dy))
        for dx in range(NX) for dc in range(NC) for dy in range(NY) if (dx, dc, dy) != (0, 0, 0)
    ]
    barrier = pltpu.get_barrier_semaphore()
    line = [at_z(d) for d in (8, 4, 12, 2, 14, 1, 15)]
    for peer in line + near_plane:
        pl.semaphore_signal(barrier, inc=1, device_id=peer, device_id_type=pl.DeviceIdType.MESH)

    for n, ref in enumerate((m_ref, v_ref)):
        mb[y, k, q, n] = jnp.concatenate(
            [ref[0, 0:8, :], ref[1, 0:8, :], ref[0, 8:16, :], ref[1, 8:16, :]], axis=1
        )
    wb[k, q] = jnp.concatenate([kw_ref[...], vw_ref[...]], axis=1).astype(bf16)

    fk = fk_ref[...].astype(f32)
    fv = fv_ref[...].astype(f32)
    rolled_k = [fk if s == 0 else pltpu.roll(fk, 32 * s, 1) for s in range(4)]
    rolled_v = [fv if s == 0 else pltpu.roll(fv, 32 * s, 1) for s in range(4)]
    lane_k = lax.broadcasted_iota(jnp.int32, (NK, 128), 1) // 32
    lane_v = lax.broadcasted_iota(jnp.int32, (NV, 128), 1) // 32
    for t in range(NY):
        cols = pl.ds(t * 128, 128)
        for half in range(2):
            at = 2 * half
            wt[pl.ds(half * NW, NK), cols] = jnp.where(lane_k == at, rolled_k[(at - t) % 4], 0.0).astype(bf16)
            wt[pl.ds(half * NW + NK, NV), cols] = jnp.where(
                lane_v == at + 1, rolled_v[(at + 1 - t) % 4], 0.0
            ).astype(bf16)

    loads[0].wait()
    loads[1].wait()
    lhs = jnp.concatenate([ck[0:HALF], cv[0:HALF], ck[HALF:TOK], cv[HALF:TOK]], axis=1)
    reduced = jnp.dot(lhs, wt[...], preferred_element_type=f32)
    for t in range(NY):
        msend[t] = reduced[:, t * 128 : (t + 1) * 128].astype(bf16)

    pl.semaphore_wait(barrier, len(line) + len(near_plane))

    sends = []
    tp = [remote(msend.at[yp(d)], yrecv.at[d - 1], y_s.at[d - 1], y_r.at[d - 1], at_y(d)) for d in (1, 2, 3)]
    for n in (1, 0, 2):
        tp[n].start()
    sends += tp
    m_far = [remote(mb.at[y, k, q], mb.at[y, k, q], mf_s.at[n], mf_r.at[n], at_z(d)) for n, d in enumerate(FAR)]
    w_far = [remote(wb.at[k, q], wb.at[k, q], wf_s.at[n], wf_r.at[n], at_z(d)) for n, d in enumerate(FAR)]
    for n in (2, 0, 1):
        m_far[n].start()
        w_far[n].start()
    sends += m_far + w_far

    loads[2].wait()
    for n in range(8):
        xt[pl.ds(n * 256, 256), :] = x_vm[:, n * 256 : (n + 1) * 256].T

    for copy in tp:
        copy.wait_recv()
    own = msend[y].astype(f32)
    for n in range(3):
        own = own + yrecv[n].astype(f32)
    swapped = pltpu.roll(own, 64, 1)
    low = lax.broadcasted_iota(jnp.int32, (HALF, 128), 1) < 64
    both = jnp.concatenate([jnp.where(low, own, swapped), jnp.where(low, swapped, own)], axis=0)
    upper = both.astype(bf16)
    lower = (both - upper.astype(f32)).astype(bf16)
    rhs = jnp.concatenate([upper, lower], axis=1)
    low_tile = lax.broadcasted_iota(jnp.int32, (16, 8, 128), 2) < 64
    for n in range(8):
        wide = jnp.dot(xt[pl.ds(n * 256, 256), :], rhs, preferred_element_type=f32)
        part = (wide[:, :128] + wide[:, 128:]).reshape(16, 2, 8, 128)
        packed = jnp.where(low_tile, part[:, 0], part[:, 1]).reshape(2, 8, 8, 128)
        for t in range(8):
            asend[t // 2, t % 2, pl.ds(n * 16, 16), :] = packed[:, t].reshape(16, 128).astype(bf16)

    to_core = remote(asend.at[:, other], crecv, c_s, c_r, partner)
    to_core.start()
    sends.append(to_core)
    to_core.wait_recv()
    for t in range(NX):
        xsend[t] = (asend[t, c].astype(f32) + crecv[t].astype(f32)).astype(bf16)
    to_x = [remote(xsend.at[xp(d)], xrecv.at[d - 1], x_s.at[d - 1], x_r.at[d - 1], at_x(d)) for d in (1, 2, 3)]
    for n in (1, 0, 2):
        to_x[n].start()
    sends += to_x

    for copy in m_far + w_far:
        copy.wait_recv()
    m_near = [remote(mb.at[y, :, q], mb.at[y, :, q], mn_s.at[n], mn_r.at[n], at_z(d)) for n, d in enumerate(NEAR)]
    w_near = [remote(wb.at[:, q], wb.at[:, q], wn_s.at[n], wn_r.at[n], at_z(d)) for n, d in enumerate(NEAR)]
    for n in (2, 0, 1):
        m_near[n].start()
    for n in (2, 0, 1):
        w_near[n].start()
    sends += m_near + w_near

    for copy in to_x:
        copy.wait_recv()
    total = xsend[x].astype(f32)
    for n in range(3):
        total = total + xrecv[n].astype(f32)
    tsend[...] = total.reshape(4, 32, 128).astype(bf16)

    near = [
        remote(tsend.at[lax.rem(zp(d), 4)], arecv.at[n], a_s.at[n], a_r.at[n], at_z(d)) for n, d in enumerate(NEAR)
    ]
    for n in (2, 0, 1):
        near[n].start()
    sends += near
    for copy in near:
        copy.wait_recv()
    quarter = tsend[q].astype(f32)
    for n in range(3):
        quarter = quarter + arecv[n].astype(f32)
    brecv[k] = quarter.astype(bf16)
    far = [remote(brecv.at[k], brecv.at[k], b_s.at[n], b_r.at[n], at_z(d)) for n, d in enumerate(FAR)]
    for n in (2, 0, 1):
        far[n].start()
    sends += far

    for copy in m_near:
        copy.wait_recv()
    m_tp = [remote(mb.at[y], mb.at[y], my_s.at[d - 1], my_r.at[d - 1], at_y(d)) for d in (1, 2, 3)]
    for n in (1, 0, 2):
        m_tp[n].start()
    sends += m_tp

    for copy in far:
        copy.wait_recv()
    quarter = brecv[0].astype(f32)
    for n in range(1, 4):
        quarter = quarter + brecv[n].astype(f32)
    gy[y, q] = quarter.astype(bf16)
    spread = [remote(gy.at[y, q], gy.at[y, q], g_s.at[n], g_r.at[n], at_z(d)) for n, d in enumerate(NEAR)]
    for n in (2, 0, 1):
        spread[n].start()
    sends += spread

    def to_tp(n, part):
        return [
            remote(gy.at[y, part], gy.at[y, part], h_s.at[n, d - 1], h_r.at[n, d - 1], at_y(d)) for d in (1, 2, 3)
        ]

    quarters = [q, lax.rem(zp(15), 4), lax.rem(zp(1), 4), lax.rem(zp(2), 4)]
    across = to_tp(0, quarters[0])
    for n in (1, 0, 2):
        across[n].start()
    for n in range(3):
        spread[n].wait_recv()
        more = to_tp(n + 1, quarters[n + 1])
        for i in (1, 0, 2):
            more[i].start()
        across += more
    sends += across

    mine = gy[y].astype(f32)
    me = (x * NC + c) * NY + y
    sb[me] = jnp.sum((mine * mine).reshape(128, 128), axis=0, keepdims=True)
    squares = [remote(sb.at[me], sb.at[me], s_s.at[n], s_r.at[n], to) for n, to in enumerate(near_plane)]
    for copy in squares:
        copy.start()
    sends += squares

    for copy in m_tp + w_near + squares + across:
        copy.wait_recv()

    sums = jnp.sum(sb[...], axis=0)
    total_sq = jnp.sum(sums, axis=1, keepdims=True)
    clip_limit = clip_target * jnp.sqrt(jnp.float32(2 * D * RANK))
    clip_factor = jnp.minimum(1.0, clip_limit / jnp.sqrt(total_sq + norm_eps))
    for t in range(NY):
        scaled = clip_factor * gy[t].astype(f32).reshape(128, 128)
        first_new = beta_first * mb[t, :, :, 0].reshape(128, 128) + (1.0 - beta_first) * scaled
        second_new = beta_second * mb[t, :, :, 1].reshape(128, 128) + (1.0 - beta_second) * scaled * scaled
        firsts[t] = first_new.reshape(16, 8, 128)
        seconds[t] = second_new.reshape(16, 8, 128)
        dirs[:, t * 128 : (t + 1) * 128] = first_new / (jnp.sqrt(second_new) + small_eps)

    left, right = at_x(3), at_x(1)
    xc_left, xc_right = xp(3) * 2 + c, xp(1) * 2 + c
    xc_across = xp(2) * 2 + c

    def block(ref, half, which):
        return ref.at[pl.ds(half * 8, 8), which]

    def pair(half, which, send, recv, n, to):
        return [
            remote(block(ref, half, which), block(ref, half, which), send.at[n, i], recv.at[n, i], to)
            for i, ref in enumerate((ko_ref, vo_ref))
        ]

    go_right, go_left, go_core = {}, {}, {}
    for half in range(2):
        direction = dirs[pl.ds(half * 64, 64), :]
        upper = direction.astype(bf16)
        lower = (direction - upper.astype(f32)).astype(bf16)
        product = lax.dot_general(
            jnp.concatenate([upper, lower], axis=0), wt[...], (((1,), (1,)), ((), ())), preferred_element_type=f32
        )
        product = product[0:64] + product[64:128]
        upd[pl.ds(half * 8, 8)] = product.reshape(8, 8, 2 * NW)
        old = wb[pl.ds(half * 2, 2)].reshape(8, 16, NW).astype(f32)
        moved = jnp.stack(
            [product[:, 0:NW].reshape(8, 8, NW), product[:, NW : 2 * NW].reshape(8, 8, NW)], axis=1
        ).reshape(8, 16, NW)
        new = (old - step_rate * moved).astype(bf16)
        ko_ref[pl.ds(half * 8, 8), xc] = new[:, :, 0:NK]
        vo_ref[pl.ds(half * 8, 8), xc] = new[:, :, NK:NW]
        if half == 0:
            go_right[0] = pair(0, xc, or_s, or_r, 0, right)
            go_core[0] = pair(0, xc, oc_s, oc_r, 0, partner)
            started = go_right[0] + go_core[0]
        else:
            go_left[0] = pair(1, xc, ol_s, ol_r, 0, left)
            go_left[1] = pair(0, xc, ol_s, ol_r, 1, left)
            go_right[1] = pair(1, xc, or_s, or_r, 1, right)
            go_core[1] = pair(1, xc, oc_s, oc_r, 1, partner)
            started = go_left[0] + go_right[1] + go_left[1] + go_core[1]
        for copy in started:
            copy.start()
        sends += started

    for out, packed_all in ((first_ref, firsts), (second_ref, seconds)):
        packed = packed_all[y, z]
        out[0, 0:8, :] = packed[:, 0:32]
        out[1, 0:8, :] = packed[:, 32:64]
        out[0, 8:16, :] = packed[:, 64:96]
        out[1, 8:16, :] = packed[:, 96:128]
    own_upd = upd[z]
    for half in range(2):
        rows = slice(half * 8, half * 8 + 8)
        at = half * NW
        nk_ref[rows, :] = kw_ref[rows, :] - step_rate * own_upd[:, at : at + NK]
        nv_ref[rows, :] = vw_ref[rows, :] - step_rate * own_upd[:, at + NK : at + NW]

    def arrived(pairs):
        for copy in pairs:
            copy.wait_recv()

    def forward(pairs):
        nonlocal sends
        for copy in pairs:
            copy.start()
        sends += pairs

    arrived(go_right[0])
    go_right[2] = pair(0, xc_left, or_s, or_r, 2, right)
    forward(go_right[2])
    go_core[2] = pair(0, xc_left, oc_s, oc_r, 2, partner)
    forward(go_core[2])
    arrived(go_left[0])
    go_left[2] = pair(1, xc_right, ol_s, ol_r, 2, left)
    forward(go_left[2])
    go_core[3] = pair(1, xc_right, oc_s, oc_r, 3, partner)
    forward(go_core[3])
    arrived(go_right[1])
    go_core[4] = pair(1, xc_left, oc_s, oc_r, 4, partner)
    forward(go_core[4])
    arrived(go_left[1])
    go_core[5] = pair(0, xc_right, oc_s, oc_r, 5, partner)
    forward(go_core[5])
    arrived(go_right[2])
    go_core[6] = pair(0, xc_across, oc_s, oc_r, 6, partner)
    forward(go_core[6])
    arrived(go_left[2])
    go_core[7] = pair(1, xc_across, oc_s, oc_r, 7, partner)
    forward(go_core[7])
    for n in range(8):
        arrived(go_core[n])
    for copy in sends:
        copy.wait_send()


def local(*args):
    vmem = pl.BlockSpec(memory_space=pltpu.VMEM)
    anywhere = pl.BlockSpec(memory_space=pl.ANY)
    dma = pltpu.SemaphoreType.DMA
    shape = jax.ShapeDtypeStruct
    outs = pl.pallas_call(
        kernel,
        out_shape=(
            shape((2, 16, 32), f32),
            shape((2, 16, 32), f32),
            shape((16, NK), f32),
            shape((16, NV), f32),
            shape((NZ, NX * NC, 16, NK), bf16),
            shape((NZ, NX * NC, 16, NV), bf16),
        ),
        in_specs=[anywhere] * 3 + [vmem] * 6,
        out_specs=[vmem] * 6,
        scratch_shapes=[
            pltpu.VMEM((TOK, D), bf16),
            pltpu.VMEM((D, TOK), bf16),
            pltpu.VMEM((TOK, NK), bf16),
            pltpu.VMEM((TOK, NV), bf16),
            pltpu.VMEM((2 * NW, 4 * 128), bf16),
            pltpu.VMEM((NY, HALF, 128), bf16),
            pltpu.VMEM((NY - 1, HALF, 128), bf16),
            pltpu.VMEM((NX, NC, 128, 128), bf16),
            pltpu.VMEM((NX, 128, 128), bf16),
            pltpu.VMEM((NX, 128, 128), bf16),
            pltpu.VMEM((NX - 1, 128, 128), bf16),
            pltpu.VMEM((4, 32, 128), bf16),
            pltpu.VMEM((3, 32, 128), bf16),
            pltpu.VMEM((4, 32, 128), bf16),
            pltpu.VMEM((NY, 4, 32, 128), bf16),
            pltpu.VMEM((NY, 4, 4, 2, 8, 128), f32),
            pltpu.VMEM((4, 4, 16, NW), bf16),
            pltpu.VMEM((NX * NC * NY, 1, 128), f32),
            pltpu.VMEM((128, 4 * 128), f32),
            pltpu.VMEM((NY, 16, 8, 128), f32),
            pltpu.VMEM((NY, 16, 8, 128), f32),
            pltpu.VMEM((16, 8, 2 * NW), f32),
            dma((3,)),
            dma((3,)), dma((3,)), dma, dma, dma((3,)), dma((3,)), dma((3,)), dma((3,)), dma((3,)), dma((3,)),
            dma((3,)), dma((3,)), dma((4, 3)), dma((4, 3)),
            dma((3,)), dma((3,)), dma((3,)), dma((3,)), dma((3,)), dma((3,)),
            dma((3,)), dma((3,)), dma((3,)), dma((3,)), dma((31,)), dma((31,)),
            dma((3, 2)), dma((3, 2)), dma((3, 2)), dma((3, 2)), dma((8, 2)), dma((8, 2)),
        ],
        compiler_params=pltpu.CompilerParams(
            collective_id=0, has_side_effects=True, vmem_limit_bytes=40 * 1024 * 1024
        ),
        name="step",
    )(*args)
    first_new, second_new, new_key, new_value, key_copy, value_copy = outs
    return first_new, second_new, new_key, new_value, key_copy.reshape(D, NK), value_copy.reshape(D, NV)


def solution(mesh):
    torus = Mesh(mesh.devices.reshape(NZ, NX, NC, NY), ("z", "x", "c", "y"))
    return jax.shard_map(
        local,
        mesh=torus,
        in_specs=(
            P(FS, None), P(FS, "y"), P(FS, "y"), P("y", None), P("y", None), P(FS, "y"), P(FS, "y"),
            P(None, FS, "y"), P(None, FS, "y"),
        ),
        out_specs=(P(None, FS, "y"), P(None, FS, "y"), P(FS, "y"), P(FS, "y"), P(None, "y"), P(None, "y")),
        check_vma=False,
    )
```

time: 270 us -> 74.4 us (0.28)
  waiting for transfers between devices: 131 us -> 0 us
  blocking collectives: 94.1 us -> 0 us
  Pallas kernels: 0 us -> 61 us
  between operations: 14.9 us -> 0.66 us
  other arithmetic: 9.92 us -> 0 us
  matrix products: 5.38 us -> 0 us
    all_gather x1 -> x0, waiting for transfers between devices: 131 us -> none  [in_one_piece(): lax.all_gather(both, axis, axis=dim, tiled=True)]
    all_to_all x6 -> x0, blocking collectives: 94.1 us -> none  [the longest x1 36.9 us: sum_by_axis(): lax.all_to_all(nearer, far, split_axis=0, concat_axis=0, tiled=True)]
    pallas_call x0 -> x1, Pallas kernels: none -> 61 us  [local(): pl.pallas_call(kernel, out_shape=(shape((2, 16, 32), f32), shape((2, 16,...]
    unnamed x18 -> x24, local copies, waits for them, and re-layouts: 3.98 us -> 12.2 us
    dot_general x5 -> x0, matrix products: 5.38 us -> none  [the longest x1 1.48 us: local(): lax.dot_general(full_direction[0], key_factor.astype(jnp.float32), back,...]
    all_to_all x3 -> x0, other arithmetic: 5.16 us -> none  [the longest x1 3.21 us: summed_on_arrival(): lax.all_to_all(in_blocks(value, dim, count), axis, 0, 0, tiled=True)]
    split x2 -> x0, local copies, waits for them, and re-layouts: 4.13 us -> none  [in_one_piece(): jnp.split(lax.all_gather(both, axis, axis=dim, tiled=True), ends, axis=al...]
    reduce_sum x6 -> x0, other arithmetic: 3.41 us -> none  [the longest x2 1.43 us: summed_on_arrival(): return jnp.sum(pieces, axis=0)]
  transfers between devices with their start and end apart: 1 -> 0, of which waited for: 1 -> 0; matrix products, arithmetic and copies ran while one was open for 0% -> 0% of each run, Pallas kernels for 0% -> 0%
where the time goes in v1:
time: 74.4 us; the launch traced here: 73.9 us
  Pallas kernels  61 us (82%)
  local copies, waits for them, and re-layouts  12.2 us (16%)
    pallas_call x1, Pallas kernels, local(): pl.pallas_call(kernel, out_shape=(shape((2, 16, 32), f32), shape((2, 16,...  61 us
    unnamed x24, local copies, waits for them, and re-layouts  12.2 us

profile of v1, /device:TPU:1, one launch (start us, length us, event | category | flops | bytes accessed | tf_op | source)
XLA Modules:
  0.0 73.9 jit_solution(1716206668186710676)
XLA Ops:
  0.6 0.0 copy-start
  0.6 1.7 %copy-done = bf16[640,2048]{1,0:T(8,128)(2,1)S(1)} copy-done((bf16[640,2048]{1,0:T(8,128)(2,1)S(1)}, bf16[640,2048]{1,0:T(8,128)(2,1)}, u32[]{:S(2)}) %copy-start) | copy-done | bytes 2621464
  2.4 0.0 copy-start.1
  2.4 1.0 %copy-done.1 = bf16[640,256]{1,0:T(8,128)(2,1)S(1)} copy-done((bf16[640,256]{1,0:T(8,128)(2,1)S(1)}, bf16[640,256]{1,0:T(8,128)(2,1)}, u32[]{:S(2)}) %copy-start.1) | copy-done | bytes 327704
  3.3 0.0 copy-start.2
  3.4 0.9 %copy-done.2 = bf16[640,128]{1,0:T(8,128)(2,1)S(1)} copy-done((bf16[640,128]{1,0:T(8,128)(2,1)S(1)}, bf16[640,128]{1,0:T(8,128)(2,1)}, u32[]{:S(2)}) %copy-start.2) | copy-done | bytes 163864
  4.3 0.0 copy-start.3
  4.3 0.8 %copy-done.3 = bf16[256,128]{1,0:T(8,128)(2,1)S(1)} copy-done((bf16[256,128]{1,0:T(8,128)(2,1)S(1)}, bf16[256,128]{1,0:T(8,128)(2,1)}, u32[]{:S(2)}) %copy-start.3) | copy-done | bytes 65560
  5.1 0.0 copy-start.4
  5.1 0.8 %copy-done.4 = bf16[128,128]{1,0:T(8,128)(2,1)S(1)} copy-done((bf16[128,128]{1,0:T(8,128)(2,1)S(1)}, bf16[128,128]{1,0:T(8,128)(2,1)}, u32[]{:S(2)}) %copy-start.4) | copy-done | bytes 32792
  5.9 0.0 copy-start.5
  5.9 0.7 copy-done.5
  6.6 0.0 copy-start.6
  6.6 0.7 copy-done.6
  7.3 0.0 copy-start.7
  7.3 0.7 copy-done.7
  8.0 0.0 copy-start.8
  8.0 0.7 copy-done.8
  8.7 61.0 %step.1 = (f32[2,16,32]{2,1,0:T(8,128)S(1)}, f32[2,16,32]{2,1,0:T(8,128)S(1)}, f32[16,128]{1,0:T(8,128)S(1)}, f32[16,256]{1,0:T(8,128)S(1)}, bf16[16,8,16,128]{3...) custom-call(bf16[640,2048]{1,0:T(8,128)(2,1)S(1)} %copy-done, bf16[640,128]{1,0:T(8,128)(2,1)S(1)} %copy-done.2, ...), custom_call_target="tpu_custom_call" | custom-call | tf_op jit(solution)/shard_map/step/pallas_call | solution.py:356
  69.7 0.6 copy.21
  70.3 0.6 copy.22
  70.9 0.6 copy.23
  71.5 0.6 copy.24
  72.2 0.8 %copy.25 = bf16[2048,128]{1,0:T(8,128)(2,1)} copy(bf16[2048,128]{1,0:T(8,128)(2,1)S(1)} %bitcast.3) | data formatting | bytes 1048576
  72.9 1.0 %copy.26 = bf16[2048,256]{1,0:T(8,128)(2,1)} copy(bf16[2048,256]{1,0:T(8,128)(2,1)S(1)} %bitcast.2) | data formatting | bytes 2097152
Async XLA Ops:
  0.6 1.7 %copy-start = (bf16[640,2048]{1,0:T(8,128)(2,1)S(1)}, bf16[640,2048]{1,0:T(8,128)(2,1)}, u32[]{:S(2)}) copy-start(bf16[640,2048]{1,0:T(8,128)(2,1)} %x_hbm.1) | copy-start | bytes 7864324
  2.4 1.0 %copy-start.1 = (bf16[640,256]{1,0:T(8,128)(2,1)S(1)}, bf16[640,256]{1,0:T(8,128)(2,1)}, u32[]{:S(2)}) copy-start(bf16[640,256]{1,0:T(8,128)(2,1)} %cv_hbm.1) | copy-start | bytes 983044
  3.3 0.9 %copy-start.2 = (bf16[640,128]{1,0:T(8,128)(2,1)S(1)}, bf16[640,128]{1,0:T(8,128)(2,1)}, u32[]{:S(2)}) copy-start(bf16[640,128]{1,0:T(8,128)(2,1)} %ck_hbm.1) | copy-start | bytes 491524
  4.3 0.8 %copy-start.3 = (bf16[256,128]{1,0:T(8,128)(2,1)S(1)}, bf16[256,128]{1,0:T(8,128)(2,1)}, u32[]{:S(2)}) copy-start(bf16[256,128]{1,0:T(8,128)(2,1)} %fv_ref.1) | copy-start | bytes 196612
  5.1 0.8 %copy-start.4 = (bf16[128,128]{1,0:T(8,128)(2,1)S(1)}, bf16[128,128]{1,0:T(8,128)(2,1)}, u32[]{:S(2)}) copy-start(bf16[128,128]{1,0:T(8,128)(2,1)} %fk_ref.1) | copy-start | bytes 98308
  5.9 0.7 copy-start.5
  6.6 0.7 copy-start.6
  7.3 0.7 copy-start.7
  8.0 0.7 copy-start.8

commit v2 on v1

--- a/solution.py
+++ b/solution.py
@@ -30,10 +30,10 @@
 
 
 def kernel(
-    x_hbm, ck_hbm, cv_hbm, fk_ref, fv_ref, kw_ref, vw_ref, m_ref, v_ref,
+    x_hbm, ck_hbm, cv_hbm, fk_hbm, fv_hbm, kw_hbm, vw_hbm, m_hbm, v_hbm,
     first_ref, second_ref, nk_ref, nv_ref, ko_ref, vo_ref,
     x_vm, xt, ck, cv, wt, msend, yrecv, asend, crecv, xsend, xrecv, tsend, arecv, brecv, gy, mb, wb, sb,
-    dirs, firsts, seconds, upd,
+    dirs, firsts, seconds, upd, fk_ref, fv_ref, kw_ref, vw_ref, m_ref, v_ref,
     in_sem, y_s, y_r, c_s, c_r, x_s, x_r, a_s, a_r, b_s, b_r, g_s, g_r, h_s, h_r,
     mf_s, mf_r, mn_s, mn_r, my_s, my_r, wf_s, wf_r, wn_s, wn_r, s_s, s_r,
     or_s, or_r, ol_s, ol_r, oc_s, oc_r,
@@ -70,9 +70,11 @@
         )
 
     loads = [
-        pltpu.make_async_copy(ck_hbm, ck, in_sem.at[0]),
-        pltpu.make_async_copy(cv_hbm, cv, in_sem.at[1]),
-        pltpu.make_async_copy(x_hbm, x_vm, in_sem.at[2]),
+        pltpu.make_async_copy(src, dst, in_sem.at[n])
+        for n, (src, dst) in enumerate([
+            (fk_hbm, fk_ref), (fv_hbm, fv_ref), (ck_hbm, ck), (cv_hbm, cv),
+            (m_hbm, m_ref), (v_hbm, v_ref), (kw_hbm, kw_ref), (vw_hbm, vw_ref), (x_hbm, x_vm),
+        ])
     ]
     for load in loads:
         load.start()
@@ -85,12 +87,9 @@
     for peer in line + near_plane:
         pl.semaphore_signal(barrier, inc=1, device_id=peer, device_id_type=pl.DeviceIdType.MESH)
 
-    for n, ref in enumerate((m_ref, v_ref)):
-        mb[y, k, q, n] = jnp.concatenate(
-            [ref[0, 0:8, :], ref[1, 0:8, :], ref[0, 8:16, :], ref[1, 8:16, :]], axis=1
-        )
-    wb[k, q] = jnp.concatenate([kw_ref[...], vw_ref[...]], axis=1).astype(bf16)
-
+    with jax.named_scope("w_factor"):
+        loads[0].wait()
+        loads[1].wait()
     fk = fk_ref[...].astype(f32)
     fv = fv_ref[...].astype(f32)
     rolled_k = [fk if s == 0 else pltpu.roll(fk, 32 * s, 1) for s in range(4)]
@@ -106,14 +105,24 @@
                 lane_v == at + 1, rolled_v[(at + 1 - t) % 4], 0.0
             ).astype(bf16)
 
-    loads[0].wait()
-    loads[1].wait()
+    with jax.named_scope("w_cot"):
+        loads[2].wait()
+        loads[3].wait()
     lhs = jnp.concatenate([ck[0:HALF], cv[0:HALF], ck[HALF:TOK], cv[HALF:TOK]], axis=1)
     reduced = jnp.dot(lhs, wt[...], preferred_element_type=f32)
     for t in range(NY):
         msend[t] = reduced[:, t * 128 : (t + 1) * 128].astype(bf16)
 
-    pl.semaphore_wait(barrier, len(line) + len(near_plane))
+    for load in loads[4:8]:
+        load.wait()
+    for n, ref in enumerate((m_ref, v_ref)):
+        mb[y, k, q, n] = jnp.concatenate(
+            [ref[0, 0:8, :], ref[1, 0:8, :], ref[0, 8:16, :], ref[1, 8:16, :]], axis=1
+        )
+    wb[k, q] = jnp.concatenate([kw_ref[...], vw_ref[...]], axis=1).astype(bf16)
+
+    with jax.named_scope("w_barrier"):
+        pl.semaphore_wait(barrier, len(line) + len(near_plane))
 
     sends = []
     tp = [remote(msend.at[yp(d)], yrecv.at[d - 1], y_s.at[d - 1], y_r.at[d - 1], at_y(d)) for d in (1, 2, 3)]
@@ -127,12 +136,13 @@
         w_far[n].start()
     sends += m_far + w_far
 
-    loads[2].wait()
+    loads[8].wait()
     for n in range(8):
         xt[pl.ds(n * 256, 256), :] = x_vm[:, n * 256 : (n + 1) * 256].T
 
-    for copy in tp:
-        copy.wait_recv()
+    with jax.named_scope("w_tp"):
+        for copy in tp:
+            copy.wait_recv()
     own = msend[y].astype(f32)
     for n in range(3):
         own = own + yrecv[n].astype(f32)
@@ -153,7 +163,8 @@
     to_core = remote(asend.at[:, other], crecv, c_s, c_r, partner)
     to_core.start()
     sends.append(to_core)
-    to_core.wait_recv()
+    with jax.named_scope("w_core"):
+        to_core.wait_recv()
     for t in range(NX):
         xsend[t] = (asend[t, c].astype(f32) + crecv[t].astype(f32)).astype(bf16)
     to_x = [remote(xsend.at[xp(d)], xrecv.at[d - 1], x_s.at[d - 1], x_r.at[d - 1], at_x(d)) for d in (1, 2, 3)]
@@ -161,8 +172,9 @@
         to_x[n].start()
     sends += to_x
 
-    for copy in m_far + w_far:
-        copy.wait_recv()
+    with jax.named_scope("w_bg_far"):
+        for copy in m_far + w_far:
+            copy.wait_recv()
     m_near = [remote(mb.at[y, :, q], mb.at[y, :, q], mn_s.at[n], mn_r.at[n], at_z(d)) for n, d in enumerate(NEAR)]
     w_near = [remote(wb.at[:, q], wb.at[:, q], wn_s.at[n], wn_r.at[n], at_z(d)) for n, d in enumerate(NEAR)]
     for n in (2, 0, 1):
@@ -171,8 +183,9 @@
         w_near[n].start()
     sends += m_near + w_near
 
-    for copy in to_x:
-        copy.wait_recv()
+    with jax.named_scope("w_x"):
+        for copy in to_x:
+            copy.wait_recv()
     total = xsend[x].astype(f32)
     for n in range(3):
         total = total + xrecv[n].astype(f32)
@@ -184,8 +197,9 @@
     for n in (2, 0, 1):
         near[n].start()
     sends += near
-    for copy in near:
-        copy.wait_recv()
+    with jax.named_scope("w_a"):
+        for copy in near:
+            copy.wait_recv()
     quarter = tsend[q].astype(f32)
     for n in range(3):
         quarter = quarter + arecv[n].astype(f32)
@@ -195,15 +209,17 @@
         far[n].start()
     sends += far
 
-    for copy in m_near:
-        copy.wait_recv()
+    with jax.named_scope("w_bg_near"):
+        for copy in m_near:
+            copy.wait_recv()
     m_tp = [remote(mb.at[y], mb.at[y], my_s.at[d - 1], my_r.at[d - 1], at_y(d)) for d in (1, 2, 3)]
     for n in (1, 0, 2):
         m_tp[n].start()
     sends += m_tp
 
-    for copy in far:
-        copy.wait_recv()
+    with jax.named_scope("w_b"):
+        for copy in far:
+            copy.wait_recv()
     quarter = brecv[0].astype(f32)
     for n in range(1, 4):
         quarter = quarter + brecv[n].astype(f32)
@@ -223,7 +239,8 @@
     for n in (1, 0, 2):
         across[n].start()
     for n in range(3):
-        spread[n].wait_recv()
+        with jax.named_scope(f"w_c{n}"):
+            spread[n].wait_recv()
         more = to_tp(n + 1, quarters[n + 1])
         for i in (1, 0, 2):
             more[i].start()
@@ -238,8 +255,15 @@
         copy.start()
     sends += squares
 
-    for copy in m_tp + w_near + squares + across:
-        copy.wait_recv()
+    with jax.named_scope("w_bg_y"):
+        for copy in m_tp + w_near:
+            copy.wait_recv()
+    with jax.named_scope("w_y"):
+        for copy in across:
+            copy.wait_recv()
+    with jax.named_scope("w_s"):
+        for copy in squares:
+            copy.wait_recv()
 
     sums = jnp.sum(sb[...], axis=0)
     total_sq = jnp.sum(sums, axis=1, keepdims=True)
@@ -320,37 +344,55 @@
             copy.start()
         sends += pairs
 
-    arrived(go_right[0])
+    with jax.named_scope("w_o0"):
+        arrived(go_right[0])
     go_right[2] = pair(0, xc_left, or_s, or_r, 2, right)
     forward(go_right[2])
     go_core[2] = pair(0, xc_left, oc_s, oc_r, 2, partner)
     forward(go_core[2])
-    arrived(go_left[0])
+    with jax.named_scope("w_o1"):
+        arrived(go_left[0])
     go_left[2] = pair(1, xc_right, ol_s, ol_r, 2, left)
     forward(go_left[2])
     go_core[3] = pair(1, xc_right, oc_s, oc_r, 3, partner)
     forward(go_core[3])
-    arrived(go_right[1])
+    with jax.named_scope("w_o2"):
+        arrived(go_right[1])
     go_core[4] = pair(1, xc_left, oc_s, oc_r, 4, partner)
     forward(go_core[4])
-    arrived(go_left[1])
+    with jax.named_scope("w_o3"):
+        arrived(go_left[1])
     go_core[5] = pair(0, xc_right, oc_s, oc_r, 5, partner)
     forward(go_core[5])
-    arrived(go_right[2])
+    with jax.named_scope("w_o4"):
+        arrived(go_right[2])
     go_core[6] = pair(0, xc_across, oc_s, oc_r, 6, partner)
     forward(go_core[6])
-    arrived(go_left[2])
+    with jax.named_scope("w_o5"):
+        arrived(go_left[2])
     go_core[7] = pair(1, xc_across, oc_s, oc_r, 7, partner)
     forward(go_core[7])
-    for n in range(8):
-        arrived(go_core[n])
-    for copy in sends:
-        copy.wait_send()
+    with jax.named_scope("w_oc"):
+        for n in range(8):
+            arrived(go_core[n])
+    with jax.named_scope("w_sends"):
+        for copy in sends:
+            copy.wait_send()
+
+
+def store(*refs):
+    sems = refs[-1]
+    count = (len(refs) - 1) // 2
+    copies = [pltpu.make_async_copy(refs[n], refs[count + n], sems.at[n]) for n in range(count)]
+    for copy in reversed(copies):
+        copy.start()
+    for copy in copies:
+        copy.wait()
 
 
 def local(*args):
     vmem = pl.BlockSpec(memory_space=pltpu.VMEM)
-    anywhere = pl.BlockSpec(memory_space=pl.ANY)
+    hbm = pl.BlockSpec(memory_space=pltpu.HBM)
     dma = pltpu.SemaphoreType.DMA
     shape = jax.ShapeDtypeStruct
     outs = pl.pallas_call(
@@ -363,7 +405,7 @@
             shape((NZ, NX * NC, 16, NK), bf16),
             shape((NZ, NX * NC, 16, NV), bf16),
         ),
-        in_specs=[anywhere] * 3 + [vmem] * 6,
+        in_specs=[hbm] * 9,
         out_specs=[vmem] * 6,
         scratch_shapes=[
             pltpu.VMEM((TOK, D), bf16),
@@ -388,7 +430,13 @@
             pltpu.VMEM((NY, 16, 8, 128), f32),
             pltpu.VMEM((NY, 16, 8, 128), f32),
             pltpu.VMEM((16, 8, 2 * NW), f32),
-            dma((3,)),
+            pltpu.VMEM((NK, RANK), bf16),
+            pltpu.VMEM((NV, RANK), bf16),
+            pltpu.VMEM((16, NK), f32),
+            pltpu.VMEM((16, NV), f32),
+            pltpu.VMEM((2, 16, 32), f32),
+            pltpu.VMEM((2, 16, 32), f32),
+            dma((9,)),
             dma((3,)), dma((3,)), dma, dma, dma((3,)), dma((3,)), dma((3,)), dma((3,)), dma((3,)), dma((3,)),
             dma((3,)), dma((3,)), dma((4, 3)), dma((4, 3)),
             dma((3,)), dma((3,)), dma((3,)), dma((3,)), dma((3,)), dma((3,)),
@@ -399,9 +447,17 @@
             collective_id=0, has_side_effects=True, vmem_limit_bytes=40 * 1024 * 1024
         ),
         name="step",
-    )(*args)
-    first_new, second_new, new_key, new_value, key_copy, value_copy = outs
-    return first_new, second_new, new_key, new_value, key_copy.reshape(D, NK), value_copy.reshape(D, NV)
+    )(*[pltpu.with_memory_space_constraint(a, pltpu.HBM) for a in args])
+    results = (*outs[:4], outs[4].reshape(D, NK), outs[5].reshape(D, NV))
+    return pl.pallas_call(
+        store,
+        out_shape=tuple(shape(r.shape, r.dtype) for r in results),
+        in_specs=[pl.BlockSpec(memory_space=pl.ANY)] * 6,
+        out_specs=[hbm] * 6,
+        scratch_shapes=[dma((6,))],
+        compiler_params=pltpu.CompilerParams(vmem_limit_bytes=1024 * 1024),
+        name="store",
+    )(*results)
 
 
 def solution(mesh):

time: 74.4 us -> 62.5 us (0.84)
  local copies, waits for them, and re-layouts: 12.2 us -> 0 us
  Pallas kernels: 61 us -> 61.8 us
    unnamed x24 -> x0, local copies, waits for them, and re-layouts: 12.2 us -> none
    pallas_call x0 -> x1, Pallas kernels: none -> 1.2 us  [local(): pl.pallas_call(store, out_shape=tuple((shape(r.shape, r.dtype) for r in r...]
where the time goes in v2:
time: 62.5 us; the launch traced here: 62.4 us
  Pallas kernels  61.8 us (99%)
  between operations  0.64 us (1%)
    pallas_call x1, Pallas kernels, local(): pl.pallas_call(kernel, out_shape=(shape((2, 16, 32), f32), shape((2, 16,...  60.6 us

profile of v2, /device:TPU:1, one launch (start us, length us, event | category | flops | bytes accessed | tf_op | source)
XLA Modules:
  0.0 62.4 jit_solution(14959271736767517739)
XLA Ops:
  0.6 60.6 %step.1 = (f32[2,16,32]{2,1,0:T(8,128)S(1)}, f32[2,16,32]{2,1,0:T(8,128)S(1)}, f32[16,128]{1,0:T(8,128)S(1)}, f32[16,256]{1,0:T(8,128)S(1)}, bf16[16,8,16,128]{3...) custom-call(bf16[640,2048]{1,0:T(8,128)(2,1)} %x_hbm.1, bf16[640,128]{1,0:T(8,128)(2,1)} %ck_hbm.1, ...), custom_call_target="tpu_custom_call" | custom-call | tf_op jit(solution)/shard_map/step/pallas_call | solution.py:398
  61.2 1.2 %store.1 = (f32[2,16,32]{2,1,0:T(8,128)}, f32[2,16,32]{2,1,0:T(8,128)}, f32[16,128]{1,0:T(8,128)}, f32[16,256]{1,0:T(8,128)}, bf16[2048,128]{1,0:T(8,128)(2,1)}, /*index=5*/bf16[2048,256]{1,0:T(8,128)(2,1)}) custom-call(f32[2,16,32]{2,1,0:T(8,128)S(1)} %get-tuple-element.12.refs_0_, f32[2,16,32]{2,1,0:T(8,128)S(1)} %get-tuple-element.13.refs_1_, ...), custom_call_target="tpu_custom_call" | custom-call | tf_op jit(solution)/shard_map/store/pallas_call | solution.py:452

commit v3 on v2

v3 whole, which is shorter than its diff:
```python
import jax
import jax.numpy as jnp
from jax import lax
from jax.experimental import pallas as pl
from jax.experimental.pallas import tpu as pltpu
from jax.sharding import Mesh
from jax.sharding import PartitionSpec as P

D = 2048
RANK = 128
NZ, NX, NC, NY = 16, 4, 2, 4
FS = ("z", "x", "c")
TOK = 640
HALF = TOK // 2
NK = 128
NV = 256
NW = NK + NV

step_rate = 0.05
clip_target = 0.1
beta_first = 0.8
beta_second = 0.95
small_eps = 1e-08
norm_eps = 1e-06

FAR = (4, 12, 8)
f32 = jnp.float32
bf16 = jnp.bfloat16


def kernel(
    x_hbm, ck_hbm, cv_hbm, fk_hbm, fv_hbm, kw_hbm, vw_hbm, m_hbm, v_hbm,
    first_ref, second_ref, nk_ref, nv_ref, ko_ref, vo_ref,
    x_vm, xt, ckv, fkv, kvw, mv, wt, msend, yrecv, asend, crecv, xsend, xrecv, tsend, arecv, brecv, gy, mb, wb, s1b, s2b,
    firsts, seconds, upd,
    in_sem, c_s, c_r, x_s, x_r, g_r, o_s, o_r, one_s, one_r,
):
    z, x, c, y = (lax.axis_index(n) for n in ("z", "x", "c", "y"))
    k, q = lax.div(z, 4), lax.rem(z, 4)
    other = 1 - c
    xc = x * 2 + c

    def zp(d):
        return lax.rem(z + d, NZ)

    def xp(d):
        return lax.rem(x + d, NX)

    def yp(d):
        return lax.rem(y + d, NY)

    def at_z(d):
        return (zp(d), x, c, y)

    def at_x(d):
        return (z, xp(d), c, y)

    def at_y(d):
        return (z, x, c, yp(d))

    partner = (z, x, other, y)

    def remote(src, dst, send, recv, to):
        return pltpu.make_async_remote_copy(
            src_ref=src, dst_ref=dst, send_sem=send, recv_sem=recv,
            device_id=to, device_id_type=pl.DeviceIdType.MESH,
        )

    names = ("tp", "a", "b", "g", "h", "s1", "s2", "mf", "mn", "my", "wf", "wn")
    send_sem = {name: one_s.at[n] for n, name in enumerate(names)}
    recv_sem = {name: one_r.at[n] for n, name in enumerate(names)}
    finish = []

    def stage(name, copies, whole):
        made = [remote(src, dst, send_sem[name], recv_sem[name], to) for src, dst, to in copies]
        for copy in made:
            copy.start()
        total = remote(whole, whole, send_sem[name], recv_sem[name], partner)
        finish.append(total)
        return total

    load_f = [pltpu.make_async_copy(fk_hbm, fkv.at[pl.ds(0, NK)], in_sem.at[0]),
              pltpu.make_async_copy(fv_hbm, fkv.at[pl.ds(NK, NV)], in_sem.at[0])]
    load_c = [pltpu.make_async_copy(ck_hbm, ckv.at[:, pl.ds(0, NK)], in_sem.at[1]),
              pltpu.make_async_copy(cv_hbm, ckv.at[:, pl.ds(NK, NV)], in_sem.at[1])]
    load_x = pltpu.make_async_copy(x_hbm, x_vm, in_sem.at[2])
    load_m = [pltpu.make_async_copy(m_hbm, mv.at[0], in_sem.at[3]),
              pltpu.make_async_copy(v_hbm, mv.at[1], in_sem.at[3])]
    load_w = [pltpu.make_async_copy(kw_hbm, kvw.at[:, pl.ds(0, NK)], in_sem.at[4]),
              pltpu.make_async_copy(vw_hbm, kvw.at[:, pl.ds(NK, NV)], in_sem.at[4])]

    for load in load_f + load_c:
        load.start()
    plane = [
        (z, xp(dx), c if dc == 0 else other, y)
        for dx in range(NX) for dc in range(NC) if (dx, dc) != (0, 0)
    ]
    around = [(zp(dz), x, c, yp(dy)) for dz in (14, 1, 15, 0) for dy in (2, 1, 3, 0) if (dz, dy) != (0, 0)]
    sources = plane + [at_z(d) for d in FAR]
    sources += [(zp(dz), x, c, yp(dy)) for dz in (2, 15, 1, 0) for dy in range(NY) if (dz, dy) != (0, 0)]
    barrier = pltpu.get_barrier_semaphore()
    for peer in sources:
        pl.semaphore_signal(barrier, inc=1, device_id=peer, device_id_type=pl.DeviceIdType.MESH)
    for load in load_m + load_w + [load_x]:
        load.start()

    with jax.named_scope("w_factor"):
        pltpu.make_async_copy(fkv, fkv, in_sem.at[0]).wait()
    factor = fkv[...].astype(f32)
    rolled = [factor if s == 0 else pltpu.roll(factor, 32 * s, 1) for s in range(4)]
    lane_group = lax.broadcasted_iota(jnp.int32, (NW, 128), 1) // 32
    is_value = (lax.broadcasted_iota(jnp.int32, (NW, 128), 0) >= NK).astype(jnp.int32)
    for half in range(2):
        keep = lane_group == 2 * half + is_value
        for t in range(NY):
            at = (2 * half - t) % 4
            placed = jnp.concatenate([rolled[at][0:NK], rolled[(at + 1) % 4][NK:NW]], axis=0)
            wt[pl.ds(half * NW, NW), pl.ds(t * 128, 128)] = jnp.where(keep, placed, 0.0).astype(bf16)

    with jax.named_scope("w_cot"):
        pltpu.make_async_copy(ckv, ckv, in_sem.at[1]).wait()
    lhs = jnp.concatenate([ckv[0:HALF], ckv[HALF:TOK]], axis=1)
    reduced = jnp.dot(lhs, wt[...], preferred_element_type=f32)
    for t in range(NY):
        msend[t] = reduced[:, t * 128 : (t + 1) * 128].astype(bf16)

    pltpu.make_async_copy(mv, mv, in_sem.at[3]).wait()
    pltpu.make_async_copy(kvw, kvw, in_sem.at[4]).wait()
    for n in range(2):
        mb[y, k, q, n] = jnp.concatenate(
            [mv[n, 0, 0:8, :], mv[n, 1, 0:8, :], mv[n, 0, 8:16, :], mv[n, 1, 8:16, :]], axis=1
        )
    wb[k, q] = kvw[...].astype(bf16)

    with jax.named_scope("w_barrier"):
        pl.semaphore_wait(barrier, len(sources))

    tp = stage("tp", [(msend.at[yp(d)], yrecv.at[d - 1], at_y(d)) for d in (2, 1, 3)], yrecv)
    m_far = stage("mf", [(mb.at[y, k, q], mb.at[y, k, q], at_z(d)) for d in (8, 4, 12)], mb.at[0, 0, pl.ds(0, 3)])
    w_far = stage("wf", [(wb.at[k, q], wb.at[k, q], at_z(d)) for d in (8, 4, 12)], wb.at[0, pl.ds(0, 3)])

    load_x.wait()
    for n in range(8):
        xt[pl.ds(n * 256, 256), :] = x_vm[:, n * 256 : (n + 1) * 256].T

    with jax.named_scope("w_tp"):
        tp.wait_recv()
    own = msend[y].astype(f32)
    for n in range(3):
        own = own + yrecv[n].astype(f32)
    swapped = pltpu.roll(own, 64, 1)
    low = lax.broadcasted_iota(jnp.int32, (HALF, 128), 1) < 64
    both = jnp.concatenate([jnp.where(low, own, swapped), jnp.where(low, swapped, own)], axis=0)
    upper = both.astype(bf16)
    lower = (both - upper.astype(f32)).astype(bf16)
    rhs = jnp.concatenate([upper, lower], axis=1)
    low_tile = lax.broadcasted_iota(jnp.int32, (16, 8, 128), 2) < 64

    order = (14, 1, 15, 0)
    quarters = [lax.rem(zp(d), 4) for d in order]

    def product_of(n):
        for half in range(2):
            rows = pl.ds(pl.multiple_of(quarters[n] * 512 + half * 256, 256), 256)
            wide = jnp.dot(xt[rows, :], rhs, preferred_element_type=f32)
            part = (wide[:, :128] + wide[:, 128:]).reshape(16, 2, 8, 128)
            packed = jnp.where(low_tile, part[:, 0], part[:, 1]).reshape(2, 8, 8, 128)
            for t in range(8):
                asend[n, t // 2, t % 2, pl.ds(half * 16, 16), :] = packed[:, t].reshape(16, 128).astype(bf16)
        copy = remote(asend.at[n, :, other], crecv.at[n], c_s.at[n], c_r.at[n], partner)
        copy.start()
        return copy

    to_core, to_x = [], []

    def core_to_x(n):
        with jax.named_scope(f"w_core{n}"):
            to_core[n].wait_recv()
        for t in range(NX):
            xsend[n, t] = (asend[n, t, c].astype(f32) + crecv[n, t].astype(f32)).astype(bf16)
        for d in (2, 1, 3):
            remote(xsend.at[n, xp(d)], xrecv.at[n, d - 1], x_s.at[n], x_r.at[n], at_x(d)).start()
        to_x.append(remote(xrecv.at[n], xrecv.at[n], x_s.at[n], x_r.at[n], partner))

    to_core.append(product_of(0))
    for n in range(1, 4):
        to_core.append(product_of(n))
        core_to_x(n - 1)
    core_to_x(3)

    with jax.named_scope("w_bg_far"):
        m_far.wait_recv()
    m_near = stage("mn", [(mb.at[y, :, q], mb.at[y, :, q], at_z(d)) for d in (14, 1, 15)], mb.at[0, pl.ds(0, 3)])

    near = []
    for n in range(4):
        with jax.named_scope(f"w_x{n}"):
            to_x[n].wait_recv()
        total = xsend[n, x].astype(f32)
        for i in range(3):
            total = total + xrecv[n, i].astype(f32)
        if n < 3:
            tsend[n] = total.astype(bf16)
            remote(tsend.at[n], arecv.at[n], send_sem["a"], recv_sem["a"], at_z(order[n])).start()
    near = remote(arecv, arecv, send_sem["a"], recv_sem["a"], partner)

    with jax.named_scope("w_bg_near"):
        m_near.wait_recv()
    m_tp = stage("my", [(mb.at[y], mb.at[y], at_y(d)) for d in (2, 1, 3)], mb.at[pl.ds(0, 3)])

    with jax.named_scope("w_a"):
        near.wait_recv()
    for n in range(3):
        total = total + arecv[n].astype(f32)
    brecv[k] = total.astype(bf16)
    far = stage("b", [(brecv.at[k], brecv.at[k], at_z(d)) for d in (8, 4, 12)], brecv.at[pl.ds(0, 3)])
    with jax.named_scope("w_bg_wf"):
        w_far.wait_recv()
    with jax.named_scope("w_b"):
        far.wait_recv()
    total = brecv[0].astype(f32)
    for n in range(1, 4):
        total = total + brecv[n].astype(f32)
    rounded = total.astype(bf16)
    gy[y, q] = rounded
    rounded = rounded.astype(f32)

    s1b[xc] = jnp.sum(rounded * rounded, axis=0, keepdims=True)
    squares = stage("s1", [(s1b.at[xc], s1b.at[xc], to) for to in plane], s1b.at[pl.ds(0, 7)])

    def to_tp(part):
        return [(gy.at[y, part], gy.at[y, part], at_y(d)) for d in (2, 1, 3)]

    def start_tp(part):
        for src, dst, to in to_tp(part):
            remote(src, dst, send_sem["h"], recv_sem["h"], to).start()

    spread = [remote(gy.at[y, q], gy.at[y, q], send_sem["g"], g_r.at[n], at_z(d)) for n, d in enumerate((14, 1, 15))]
    for copy in spread:
        copy.start()
    start_tp(q)
    across = remote(gy.at[pl.ds(0, 3)], gy.at[pl.ds(0, 3)], send_sem["h"], recv_sem["h"], partner)
    for n, d in ((1, 15), (2, 1)):
        with jax.named_scope(f"w_c{n}"):
            spread[n].wait_recv()
        start_tp(lax.rem(zp(d), 4))
    with jax.named_scope("w_s1"):
        squares.wait_recv()
    row = s1b[0]
    for n in range(1, 8):
        row = row + s1b[n]
    s2b[q * 4 + y] = row
    squares_2 = stage("s2", [(s2b.at[q * 4 + y], s2b.at[q * 4 + y], to) for to in around], s2b.at[pl.ds(0, 15)])
    with jax.named_scope("w_c0"):
        spread[0].wait_recv()
    start_tp(lax.rem(zp(2), 4))
    w_near = stage("wn", [(wb.at[:, q], wb.at[:, q], at_z(d)) for d in (14, 1, 15)], wb.at[pl.ds(0, 3)])

    with jax.named_scope("w_bg_y"):
        m_tp.wait_recv()
    with jax.named_scope("w_s2"):
        squares_2.wait_recv()
    with jax.named_scope("w_y"):
        across.wait_recv()

    total_sq = jnp.sum(jnp.sum(s2b[...], axis=0), axis=1, keepdims=True)
    clip_limit = clip_target * jnp.sqrt(jnp.float32(2 * D * RANK))
    clip_factor = jnp.minimum(1.0, clip_limit / jnp.sqrt(total_sq + norm_eps))

    left, right = at_x(3), at_x(1)
    xc_left, xc_right, xc_across = xp(3) * 2 + c, xp(1) * 2 + c, xp(2) * 2 + c
    piece = wb.at[pl.ds(0, 2)]

    def pair(half, which, n, to):
        for ref in (ko_ref, vo_ref):
            at = ref.at[pl.ds(half * 8, 8), which]
            remote(at, at, o_s.at[n], o_r.at[n], to).start()
        return remote(piece, piece, o_s.at[n], o_r.at[n], to)

    def to_partner(half, which):
        for ref in (ko_ref, vo_ref):
            at = ref.at[pl.ds(half * 8, 8), which]
            remote(at, at, o_s.at[6], o_r.at[6], partner).start()

    go_right, go_left = [], []
    for half in range(2):
        pieces = []
        for t in range(NY):
            at = pl.ds(half * 2, 2)
            scaled = clip_factor * gy[t, at].astype(f32).reshape(64, 128)
            first_new = beta_first * mb[t, at, :, 0].reshape(64, 128) + (1.0 - beta_first) * scaled
            second_new = beta_second * mb[t, at, :, 1].reshape(64, 128) + (1.0 - beta_second) * scaled * scaled
            firsts[t, pl.ds(half * 8, 8)] = first_new.reshape(8, 8, 128)
            seconds[t, pl.ds(half * 8, 8)] = second_new.reshape(8, 8, 128)
            pieces.append(first_new / (jnp.sqrt(second_new) + small_eps))
        direction = jnp.concatenate(pieces, axis=1)
        upper = direction.astype(bf16)
        lower = (direction - upper.astype(f32)).astype(bf16)
        product = lax.dot_general(
            jnp.concatenate([upper, lower], axis=0), wt[...], (((1,), (1,)), ((), ())), preferred_element_type=f32
        )
        product = product[0:64] + product[64:128]
        upd[pl.ds(half * 8, 8)] = product.reshape(8, 8, 2 * NW)
        if half == 0:
            with jax.named_scope("w_bg_wn"):
                w_near.wait_recv()
        old = wb[pl.ds(half * 2, 2)].reshape(8, 16, NW).astype(f32)
        moved = jnp.stack(
            [product[:, 0:NW].reshape(8, 8, NW), product[:, NW : 2 * NW].reshape(8, 8, NW)], axis=1
        ).reshape(8, 16, NW)
        new = (old - step_rate * moved).astype(bf16)
        ko_ref[pl.ds(half * 8, 8), xc] = new[:, :, 0:NK]
        vo_ref[pl.ds(half * 8, 8), xc] = new[:, :, NK:NW]
        if half == 0:
            go_right.append(pair(0, xc, 0, right))
            to_partner(0, xc)
        else:
            go_left.append(pair(1, xc, 3, left))
            go_right.append(pair(1, xc, 1, right))
            go_left.append(pair(0, xc, 4, left))
            to_partner(1, xc)

    for out, packed_all in ((first_ref, firsts), (second_ref, seconds)):
        packed = packed_all[y, z]
        out[0, 0:8, :] = packed[:, 0:32]
        out[1, 0:8, :] = packed[:, 32:64]
        out[0, 8:16, :] = packed[:, 64:96]
        out[1, 8:16, :] = packed[:, 96:128]
    own_upd = upd[z]
    for half in range(2):
        rows = slice(half * 8, half * 8 + 8)
        at = half * NW
        nk_ref[rows, :] = kvw[rows, 0:NK] - step_rate * own_upd[:, at : at + NK]
        nv_ref[rows, :] = kvw[rows, NK:NW] - step_rate * own_upd[:, at + NK : at + NW]

    finish.append(near)
    finish.append(across)
    for copy in to_core + to_x + finish:
        copy.wait_send()
    remote(arecv, arecv, send_sem["g"], g_r.at[0], partner).wait_send()

    with jax.named_scope("w_o0"):
        go_right[0].wait_recv()
    go_right.append(pair(0, xc_left, 2, right))
    to_partner(0, xc_left)
    with jax.named_scope("w_o1"):
        go_left[0].wait_recv()
    go_left.append(pair(1, xc_right, 5, left))
    to_partner(1, xc_right)
    with jax.named_scope("w_o2"):
        go_right[1].wait_recv()
    to_partner(1, xc_left)
    with jax.named_scope("w_o3"):
        go_left[1].wait_recv()
    to_partner(0, xc_right)
    with jax.named_scope("w_o4"):
        go_right[2].wait_recv()
    to_partner(0, xc_across)
    with jax.named_scope("w_o5"):
        go_left[2].wait_recv()
    to_partner(1, xc_across)
    with jax.named_scope("w_osend"):
        for copy in go_right + go_left:
            copy.wait_send()
    with jax.named_scope("w_oc"):
        both_ways = vo_ref.at[pl.ds(0, 12)]
        last = remote(both_ways, both_ways, o_s.at[6], o_r.at[6], partner)
        last.wait_recv()
        last.wait_send()


def store(*refs):
    sems = refs[-1]
    count = (len(refs) - 1) // 2
    copies = [pltpu.make_async_copy(refs[n], refs[count + n], sems.at[n]) for n in range(count)]
    for copy in reversed(copies):
        copy.start()
    for copy in copies:
        copy.wait()


def local(*args):
    vmem = pl.BlockSpec(memory_space=pltpu.VMEM)
    hbm = pl.BlockSpec(memory_space=pltpu.HBM)
    dma = pltpu.SemaphoreType.DMA
    shape = jax.ShapeDtypeStruct
    outs = pl.pallas_call(
        kernel,
        out_shape=(
            shape((2, 16, 32), f32),
            shape((2, 16, 32), f32),
            shape((16, NK), f32),
            shape((16, NV), f32),
            shape((NZ, NX * NC, 16, NK), bf16),
            shape((NZ, NX * NC, 16, NV), bf16),
        ),
        in_specs=[hbm] * 9,
        out_specs=[vmem] * 6,
        scratch_shapes=[
            pltpu.VMEM((TOK, D), bf16),
            pltpu.VMEM((D, TOK), bf16),
            pltpu.VMEM((TOK, NW), bf16),
            pltpu.VMEM((NW, RANK), bf16),
            pltpu.VMEM((16, NW), f32),
            pltpu.VMEM((2, 2, 16, 32), f32),
            pltpu.VMEM((2 * NW, 4 * 128), bf16),
            pltpu.VMEM((NY, HALF, 128), bf16),
            pltpu.VMEM((NY - 1, HALF, 128), bf16),
            pltpu.VMEM((4, NX, NC, 32, 128), bf16),
            pltpu.VMEM((4, NX, 32, 128), bf16),
            pltpu.VMEM((4, NX, 32, 128), bf16),
            pltpu.VMEM((4, NX - 1, 32, 128), bf16),
            pltpu.VMEM((3, 32, 128), bf16),
            pltpu.VMEM((3, 32, 128), bf16),
            pltpu.VMEM((4, 32, 128), bf16),
            pltpu.VMEM((NY, 4, 32, 128), bf16),
            pltpu.VMEM((NY, 4, 4, 2, 8, 128), f32),
            pltpu.VMEM((4, 4, 16, NW), bf16),
            pltpu.VMEM((NX * NC, 1, 128), f32),
            pltpu.VMEM((4 * NY, 1, 128), f32),
            pltpu.VMEM((NY, 16, 8, 128), f32),
            pltpu.VMEM((NY, 16, 8, 128), f32),
            pltpu.VMEM((16, 8, 2 * NW), f32),
            dma((5,)), dma((4,)), dma((4,)), dma((4,)), dma((4,)), dma((3,)), dma((7,)), dma((7,)), dma((12,)), dma((12,)),
        ],
        compiler_params=pltpu.CompilerParams(
            collective_id=0, has_side_effects=True, vmem_limit_bytes=40 * 1024 * 1024
        ),
        name="step",
    )(*[pltpu.with_memory_space_constraint(a, pltpu.HBM) for a in args])
    results = (*outs[:4], outs[4].reshape(D, NK), outs[5].reshape(D, NV))
    return pl.pallas_call(
        store,
        out_shape=tuple(shape(r.shape, r.dtype) for r in results),
        in_specs=[pl.BlockSpec(memory_space=pl.ANY)] * 6,
        out_specs=[hbm] * 6,
        scratch_shapes=[dma((6,))],
        compiler_params=pltpu.CompilerParams(vmem_limit_bytes=1024 * 1024),
        name="store",
    )(*results)


def solution(mesh):
    torus = Mesh(mesh.devices.reshape(NZ, NX, NC, NY), ("z", "x", "c", "y"))
    return jax.shard_map(
        local,
        mesh=torus,
        in_specs=(
            P(FS, None), P(FS, "y"), P(FS, "y"), P("y", None), P("y", None), P(FS, "y"), P(FS, "y"),
            P(None, FS, "y"), P(None, FS, "y"),
        ),
        out_specs=(P(None, FS, "y"), P(None, FS, "y"), P(FS, "y"), P(FS, "y"), P(None, "y"), P(None, "y")),
        check_vma=False,
    )
```

time: 62.5 us -> 58.2 us (0.931)
  Pallas kernels: 61.8 us -> 57.4 us
    pallas_call x1, Pallas kernels: 60.6 us -> 56.2 us  [local(): pl.pallas_call(kernel, out_shape=(shape((2, 16, 32), f32), shape((2, 16,...]
where the time goes in v3:
time: 58.2 us; the launch traced here: 58.1 us
  Pallas kernels  57.4 us (99%)
  between operations  0.64 us (1%)
    pallas_call x1, Pallas kernels, local(): pl.pallas_call(kernel, out_shape=(shape((2, 16, 32), f32), shape((2, 16,...  56.2 us
    pallas_call x1, Pallas kernels, local(): pl.pallas_call(store, out_shape=tuple((shape(r.shape, r.dtype) for r in r...  1.2 us

profile of v3, /device:TPU:1, one launch (start us, length us, event | category | flops | bytes accessed | tf_op | source)
XLA Modules:
  0.0 58.1 jit_solution(17454088392323807928)
XLA Ops:
  0.6 56.2 %step.1 = (f32[2,16,32]{2,1,0:T(8,128)S(1)}, f32[2,16,32]{2,1,0:T(8,128)S(1)}, f32[16,128]{1,0:T(8,128)S(1)}, f32[16,256]{1,0:T(8,128)S(1)}, bf16[16,8,16,128]{3...) custom-call(bf16[640,2048]{1,0:T(8,128)(2,1)} %x_hbm.1, bf16[640,128]{1,0:T(8,128)(2,1)} %ck_hbm.1, ...), custom_call_target="tpu_custom_call" | custom-call | tf_op jit(solution)/shard_map/step/pallas_call | solution.py:387
  56.9 1.2 %store.1 = (f32[2,16,32]{2,1,0:T(8,128)}, f32[2,16,32]{2,1,0:T(8,128)}, f32[16,128]{1,0:T(8,128)}, f32[16,256]{1,0:T(8,128)}, bf16[2048,128]{1,0:T(8,128)(2,1)}, /*index=5*/bf16[2048,256]{1,0:T(8,128)(2,1)}) custom-call(f32[2,16,32]{2,1,0:T(8,128)S(1)} %get-tuple-element.12.refs_0_, f32[2,16,32]{2,1,0:T(8,128)S(1)} %get-tuple-element.13.refs_1_, ...), custom_call_target="tpu_custom_call" | custom-call | tf_op jit(solution)/shard_map/store/pallas_call | solution.py:432

commit v4 on v3

--- a/solution.py
+++ b/solution.py
@@ -31,7 +31,7 @@
 def kernel(
     x_hbm, ck_hbm, cv_hbm, fk_hbm, fv_hbm, kw_hbm, vw_hbm, m_hbm, v_hbm,
     first_ref, second_ref, nk_ref, nv_ref, ko_ref, vo_ref,
-    x_vm, xt, ckv, fkv, kvw, mv, wt, msend, yrecv, asend, crecv, xsend, xrecv, tsend, arecv, brecv, gy, mb, wb, s1b, s2b,
+    x_vm, xt, ckv, fkv, kvw, mv, wt, msend, yrecv, asend, crecv, xsend, xrecv, tsend, arecv, brecv, gy, mb, wb, sb,
     firsts, seconds, upd,
     in_sem, c_s, c_r, x_s, x_r, g_r, o_s, o_r, one_s, one_r,
 ):
@@ -66,7 +66,7 @@
             device_id=to, device_id_type=pl.DeviceIdType.MESH,
         )
 
-    names = ("tp", "a", "b", "g", "h", "s1", "s2", "mf", "mn", "my", "wf", "wn")
+    names = ("tp", "a", "b", "g", "h", "sq", "mf", "mn", "my", "wf", "wn")
     send_sem = {name: one_s.at[n] for n, name in enumerate(names)}
     recv_sem = {name: one_r.at[n] for n, name in enumerate(names)}
     finish = []
@@ -91,13 +91,7 @@
 
     for load in load_f + load_c:
         load.start()
-    plane = [
-        (z, xp(dx), c if dc == 0 else other, y)
-        for dx in range(NX) for dc in range(NC) if (dx, dc) != (0, 0)
-    ]
-    around = [(zp(dz), x, c, yp(dy)) for dz in (14, 1, 15, 0) for dy in (2, 1, 3, 0) if (dz, dy) != (0, 0)]
-    sources = plane + [at_z(d) for d in FAR]
-    sources += [(zp(dz), x, c, yp(dy)) for dz in (2, 15, 1, 0) for dy in range(NY) if (dz, dy) != (0, 0)]
+    sources = [at_z(d) for d in FAR + (2, 15, 1)] + [at_y(d) for d in (2, 1, 3)] + [at_x(d) for d in (2, 1, 3)] + [partner]
     barrier = pltpu.get_barrier_semaphore()
     for peer in sources:
         pl.semaphore_signal(barrier, inc=1, device_id=peer, device_id_type=pl.DeviceIdType.MESH)
@@ -225,8 +219,15 @@
     gy[y, q] = rounded
     rounded = rounded.astype(f32)
 
-    s1b[xc] = jnp.sum(rounded * rounded, axis=0, keepdims=True)
-    squares = stage("s1", [(s1b.at[xc], s1b.at[xc], to) for to in plane], s1b.at[pl.ds(0, 7)])
+    def spot(residue, yy, which):
+        return (residue * NY + yy) * (NX * NC) + which
+
+    mine = sb.at[spot(q, y, xc)]
+    mine[...] = jnp.sum(rounded * rounded, axis=0, keepdims=True)
+    around = sorted(
+        ((dz, dx, dc, dy) for dz in (14, 15, 1, 0) for dx in range(NX) for dc in range(NC) for dy in range(NY)),
+        key=lambda d: -(min(d[0], NZ - d[0]) + min(d[1], NX - d[1]) + min(d[3], NY - d[3]) + d[2] * 0.5),
+    )[:-1]
 
     def to_tp(part):
         return [(gy.at[y, part], gy.at[y, part], at_y(d)) for d in (2, 1, 3)]
@@ -240,17 +241,15 @@
         copy.start()
     start_tp(q)
     across = remote(gy.at[pl.ds(0, 3)], gy.at[pl.ds(0, 3)], send_sem["h"], recv_sem["h"], partner)
+    squares = stage(
+        "sq",
+        [(mine, mine, (zp(dz), xp(dx), c if dc == 0 else other, yp(dy))) for dz, dx, dc, dy in around],
+        sb.at[pl.ds(0, len(around))],
+    )
     for n, d in ((1, 15), (2, 1)):
         with jax.named_scope(f"w_c{n}"):
             spread[n].wait_recv()
         start_tp(lax.rem(zp(d), 4))
-    with jax.named_scope("w_s1"):
-        squares.wait_recv()
-    row = s1b[0]
-    for n in range(1, 8):
-        row = row + s1b[n]
-    s2b[q * 4 + y] = row
-    squares_2 = stage("s2", [(s2b.at[q * 4 + y], s2b.at[q * 4 + y], to) for to in around], s2b.at[pl.ds(0, 15)])
     with jax.named_scope("w_c0"):
         spread[0].wait_recv()
     start_tp(lax.rem(zp(2), 4))
@@ -258,40 +257,47 @@
 
     with jax.named_scope("w_bg_y"):
         m_tp.wait_recv()
-    with jax.named_scope("w_s2"):
-        squares_2.wait_recv()
     with jax.named_scope("w_y"):
         across.wait_recv()
-
-    total_sq = jnp.sum(jnp.sum(s2b[...], axis=0), axis=1, keepdims=True)
+    with jax.named_scope("w_s"):
+        squares.wait_recv()
+
+    total_sq = jnp.sum(jnp.sum(sb[...], axis=0), axis=1, keepdims=True)
     clip_limit = clip_target * jnp.sqrt(jnp.float32(2 * D * RANK))
     clip_factor = jnp.minimum(1.0, clip_limit / jnp.sqrt(total_sq + norm_eps))
 
     left, right = at_x(3), at_x(1)
     xc_left, xc_right, xc_across = xp(3) * 2 + c, xp(1) * 2 + c, xp(2) * 2 + c
-    piece = wb.at[pl.ds(0, 2)]
-
-    def pair(half, which, n, to):
+    piece = wb.at[0]
+
+    def send_piece(part, which, send, recv, to):
         for ref in (ko_ref, vo_ref):
-            at = ref.at[pl.ds(half * 8, 8), which]
-            remote(at, at, o_s.at[n], o_r.at[n], to).start()
-        return remote(piece, piece, o_s.at[n], o_r.at[n], to)
-
-    def to_partner(half, which):
-        for ref in (ko_ref, vo_ref):
-            at = ref.at[pl.ds(half * 8, 8), which]
-            remote(at, at, o_s.at[6], o_r.at[6], partner).start()
+            at = ref.at[pl.ds(part * 4, 4), which]
+            remote(at, at, send, recv, to).start()
 
     go_right, go_left = [], []
-    for half in range(2):
+
+    def to_right(part, which):
+        n = len(go_right)
+        send_piece(part, which, o_s.at[n], o_r.at[n], right)
+        go_right.append(remote(piece, piece, o_s.at[n], o_r.at[n], right))
+
+    def to_left(part, which):
+        n = 6 + len(go_left)
+        send_piece(part, which, o_s.at[n], o_r.at[n], left)
+        go_left.append(remote(piece, piece, o_s.at[n], o_r.at[n], left))
+
+    def to_partner(part, which):
+        send_piece(part, which, o_s.at[12], o_r.at[12], partner)
+
+    for part in (0, 3, 1, 2):
         pieces = []
         for t in range(NY):
-            at = pl.ds(half * 2, 2)
-            scaled = clip_factor * gy[t, at].astype(f32).reshape(64, 128)
-            first_new = beta_first * mb[t, at, :, 0].reshape(64, 128) + (1.0 - beta_first) * scaled
-            second_new = beta_second * mb[t, at, :, 1].reshape(64, 128) + (1.0 - beta_second) * scaled * scaled
-            firsts[t, pl.ds(half * 8, 8)] = first_new.reshape(8, 8, 128)
-            seconds[t, pl.ds(half * 8, 8)] = second_new.reshape(8, 8, 128)
+            scaled = clip_factor * gy[t, part].astype(f32)
+            first_new = beta_first * mb[t, part, :, 0].reshape(32, 128) + (1.0 - beta_first) * scaled
+            second_new = beta_second * mb[t, part, :, 1].reshape(32, 128) + (1.0 - beta_second) * scaled * scaled
+            firsts[t, pl.ds(part * 4, 4)] = first_new.reshape(4, 8, 128)
+            seconds[t, pl.ds(part * 4, 4)] = second_new.reshape(4, 8, 128)
             pieces.append(first_new / (jnp.sqrt(second_new) + small_eps))
         direction = jnp.concatenate(pieces, axis=1)
         upper = direction.astype(bf16)
@@ -299,26 +305,26 @@
         product = lax.dot_general(
             jnp.concatenate([upper, lower], axis=0), wt[...], (((1,), (1,)), ((), ())), preferred_element_type=f32
         )
-        product = product[0:64] + product[64:128]
-        upd[pl.ds(half * 8, 8)] = product.reshape(8, 8, 2 * NW)
-        if half == 0:
+        product = product[0:32] + product[32:64]
+        upd[pl.ds(part * 4, 4)] = product.reshape(4, 8, 2 * NW)
+        if part == 0:
             with jax.named_scope("w_bg_wn"):
                 w_near.wait_recv()
-        old = wb[pl.ds(half * 2, 2)].reshape(8, 16, NW).astype(f32)
+        old = wb[part].astype(f32)
         moved = jnp.stack(
-            [product[:, 0:NW].reshape(8, 8, NW), product[:, NW : 2 * NW].reshape(8, 8, NW)], axis=1
-        ).reshape(8, 16, NW)
+            [product[:, 0:NW].reshape(4, 8, NW), product[:, NW : 2 * NW].reshape(4, 8, NW)], axis=1
+        ).reshape(4, 16, NW)
         new = (old - step_rate * moved).astype(bf16)
-        ko_ref[pl.ds(half * 8, 8), xc] = new[:, :, 0:NK]
-        vo_ref[pl.ds(half * 8, 8), xc] = new[:, :, NK:NW]
-        if half == 0:
-            go_right.append(pair(0, xc, 0, right))
-            to_partner(0, xc)
-        else:
-            go_left.append(pair(1, xc, 3, left))
-            go_right.append(pair(1, xc, 1, right))
-            go_left.append(pair(0, xc, 4, left))
-            to_partner(1, xc)
+        ko_ref[pl.ds(part * 4, 4), xc] = new[:, :, 0:NK]
+        vo_ref[pl.ds(part * 4, 4), xc] = new[:, :, NK:NW]
+        if part != 3:
+            to_right(part, xc)
+        if part >= 2:
+            to_left(part, xc)
+        to_partner(part, xc)
+    to_left(1, xc)
+    to_right(3, xc)
+    to_left(0, xc)
 
     for out, packed_all in ((first_ref, firsts), (second_ref, seconds)):
         packed = packed_all[y, z]
@@ -339,32 +345,23 @@
         copy.wait_send()
     remote(arecv, arecv, send_sem["g"], g_r.at[0], partner).wait_send()
 
-    with jax.named_scope("w_o0"):
-        go_right[0].wait_recv()
-    go_right.append(pair(0, xc_left, 2, right))
-    to_partner(0, xc_left)
-    with jax.named_scope("w_o1"):
-        go_left[0].wait_recv()
-    go_left.append(pair(1, xc_right, 5, left))
-    to_partner(1, xc_right)
-    with jax.named_scope("w_o2"):
-        go_right[1].wait_recv()
-    to_partner(1, xc_left)
-    with jax.named_scope("w_o3"):
-        go_left[1].wait_recv()
-    to_partner(0, xc_right)
-    with jax.named_scope("w_o4"):
-        go_right[2].wait_recv()
-    to_partner(0, xc_across)
-    with jax.named_scope("w_o5"):
-        go_left[2].wait_recv()
-    to_partner(1, xc_across)
+    for n in range(6):
+        with jax.named_scope(f"w_r{n}"):
+            go_right[n].wait_recv()
+        if n < 2:
+            to_right(n, xc_left)
+        to_partner(n % 4, xc_left if n < 4 else xc_across)
+        with jax.named_scope(f"w_l{n}"):
+            go_left[n].wait_recv()
+        if n < 2:
+            to_left(3 - n, xc_right)
+        to_partner(3 - n % 4, xc_right if n < 4 else xc_across)
     with jax.named_scope("w_osend"):
         for copy in go_right + go_left:
             copy.wait_send()
     with jax.named_scope("w_oc"):
         both_ways = vo_ref.at[pl.ds(0, 12)]
-        last = remote(both_ways, both_ways, o_s.at[6], o_r.at[6], partner)
+        last = remote(both_ways, both_ways, o_s.at[12], o_r.at[12], partner)
         last.wait_recv()
         last.wait_send()
 
@@ -416,12 +413,11 @@
             pltpu.VMEM((NY, 4, 32, 128), bf16),
             pltpu.VMEM((NY, 4, 4, 2, 8, 128), f32),
             pltpu.VMEM((4, 4, 16, NW), bf16),
-            pltpu.VMEM((NX * NC, 1, 128), f32),
-            pltpu.VMEM((4 * NY, 1, 128), f32),
+            pltpu.VMEM((4 * NY * NX * NC, 1, 128), f32),
             pltpu.VMEM((NY, 16, 8, 128), f32),
             pltpu.VMEM((NY, 16, 8, 128), f32),
             pltpu.VMEM((16, 8, 2 * NW), f32),
-            dma((5,)), dma((4,)), dma((4,)), dma((4,)), dma((4,)), dma((3,)), dma((7,)), dma((7,)), dma((12,)), dma((12,)),
+            dma((5,)), dma((4,)), dma((4,)), dma((4,)), dma((4,)), dma((3,)), dma((13,)), dma((13,)), dma((11,)), dma((11,)),
         ],
         compiler_params=pltpu.CompilerParams(
             collective_id=0, has_side_effects=True, vmem_limit_bytes=40 * 1024 * 1024

time: 58.2 us -> 57.8 us (level)
  no operation moved by 1% of the time
where the time goes in v4:
time: 57.8 us; the launch traced here: 57.7 us
  Pallas kernels  57 us (99%)
  between operations  0.64 us (1%)
    pallas_call x1, Pallas kernels, local(): pl.pallas_call(kernel, out_shape=(shape((2, 16, 32), f32), shape((2, 16,...  55.8 us
    pallas_call x1, Pallas kernels, local(): pl.pallas_call(store, out_shape=tuple((shape(r.shape, r.dtype) for r in r...  1.2 us

profile of v4, /device:TPU:1, one launch (start us, length us, event | category | flops | bytes accessed | tf_op | source)
XLA Modules:
  0.0 57.7 jit_solution(1224938725452259340)
XLA Ops:
  0.6 55.8 %step.1 = (f32[2,16,32]{2,1,0:T(8,128)S(1)}, f32[2,16,32]{2,1,0:T(8,128)S(1)}, f32[16,128]{1,0:T(8,128)S(1)}, f32[16,256]{1,0:T(8,128)S(1)}, bf16[16,8,16,128]{3...) custom-call(bf16[640,2048]{1,0:T(8,128)(2,1)} %x_hbm.1, bf16[640,128]{1,0:T(8,128)(2,1)} %ck_hbm.1, ...), custom_call_target="tpu_custom_call" | custom-call | tf_op jit(solution)/shard_map/step/pallas_call | solution.py:384
  56.5 1.2 %store.1 = (f32[2,16,32]{2,1,0:T(8,128)}, f32[2,16,32]{2,1,0:T(8,128)}, f32[16,128]{1,0:T(8,128)}, f32[16,256]{1,0:T(8,128)}, bf16[2048,128]{1,0:T(8,128)(2,1)}, /*index=5*/bf16[2048,256]{1,0:T(8,128)(2,1)}) custom-call(f32[2,16,32]{2,1,0:T(8,128)S(1)} %get-tuple-element.12.refs_0_, f32[2,16,32]{2,1,0:T(8,128)S(1)} %get-tuple-element.13.refs_1_, ...), custom_call_target="tpu_custom_call" | custom-call | tf_op jit(solution)/shard_map/store/pallas_call | solution.py:428

commit v5 on v4

--- a/solution.py
+++ b/solution.py
@@ -31,9 +31,9 @@
 def kernel(
     x_hbm, ck_hbm, cv_hbm, fk_hbm, fv_hbm, kw_hbm, vw_hbm, m_hbm, v_hbm,
     first_ref, second_ref, nk_ref, nv_ref, ko_ref, vo_ref,
-    x_vm, xt, ckv, fkv, kvw, mv, wt, msend, yrecv, asend, crecv, xsend, xrecv, tsend, arecv, brecv, gy, mb, wb, sb,
+    x_vm, ckv, fkv, kvw, mv, wt, wtt, msend, yrecv, asend, crecv, xsend, xrecv, tsend, arecv, brecv, gy, mb, wb, sb,
     firsts, seconds, upd,
-    in_sem, c_s, c_r, x_s, x_r, g_r, o_s, o_r, one_s, one_r,
+    in_sem, c_s, c_r, x_s, x_r, o_s, o_r, one_s, one_r,
 ):
     z, x, c, y = (lax.axis_index(n) for n in ("z", "x", "c", "y"))
     k, q = lax.div(z, 4), lax.rem(z, 4)
@@ -134,8 +134,8 @@
     w_far = stage("wf", [(wb.at[k, q], wb.at[k, q], at_z(d)) for d in (8, 4, 12)], wb.at[0, pl.ds(0, 3)])
 
     load_x.wait()
-    for n in range(8):
-        xt[pl.ds(n * 256, 256), :] = x_vm[:, n * 256 : (n + 1) * 256].T
+    for n in range(4):
+        wtt[pl.ds(n * 128, 128), :] = wt[:, n * 128 : (n + 1) * 128].T
 
     with jax.named_scope("w_tp"):
         tp.wait_recv()
@@ -145,22 +145,22 @@
     swapped = pltpu.roll(own, 64, 1)
     low = lax.broadcasted_iota(jnp.int32, (HALF, 128), 1) < 64
     both = jnp.concatenate([jnp.where(low, own, swapped), jnp.where(low, swapped, own)], axis=0)
-    upper = both.astype(bf16)
-    lower = (both - upper.astype(f32)).astype(bf16)
-    rhs = jnp.concatenate([upper, lower], axis=1)
-    low_tile = lax.broadcasted_iota(jnp.int32, (16, 8, 128), 2) < 64
+    upper = both.astype(bf16).astype(f32)
+    first_half = lax.broadcasted_iota(jnp.int32, (TOK, 128), 1) < 64
+    stream = jnp.where(first_half, upper, both - upper).astype(bf16).T
+    low_tile = lax.broadcasted_iota(jnp.int32, (32, 8, 128), 2) < 64
 
     order = (14, 1, 15, 0)
     quarters = [lax.rem(zp(d), 4) for d in order]
 
     def product_of(n):
-        for half in range(2):
-            rows = pl.ds(pl.multiple_of(quarters[n] * 512 + half * 256, 256), 256)
-            wide = jnp.dot(xt[rows, :], rhs, preferred_element_type=f32)
-            part = (wide[:, :128] + wide[:, 128:]).reshape(16, 2, 8, 128)
-            packed = jnp.where(low_tile, part[:, 0], part[:, 1]).reshape(2, 8, 8, 128)
-            for t in range(8):
-                asend[n, t // 2, t % 2, pl.ds(half * 16, 16), :] = packed[:, t].reshape(16, 128).astype(bf16)
+        cols = pl.ds(pl.multiple_of(quarters[n] * 512, 512), 512)
+        wide = jnp.dot(stream, x_vm[:, cols], preferred_element_type=f32)
+        part = wide[0:64] + wide[64:128]
+        part = jnp.concatenate([part, part], axis=0).T.reshape(32, 2, 8, 128)
+        packed = jnp.where(low_tile, part[:, 0], part[:, 1]).reshape(4, 8, 8, 128)
+        for t in range(8):
+            asend[n, t // 2, t % 2] = packed[:, t].reshape(32, 128).astype(bf16)
         copy = remote(asend.at[n, :, other], crecv.at[n], c_s.at[n], c_r.at[n], partner)
         copy.start()
         return copy
@@ -176,17 +176,13 @@
             remote(xsend.at[n, xp(d)], xrecv.at[n, d - 1], x_s.at[n], x_r.at[n], at_x(d)).start()
         to_x.append(remote(xrecv.at[n], xrecv.at[n], x_s.at[n], x_r.at[n], partner))
 
-    to_core.append(product_of(0))
+    for n in range(3):
+        to_core.append(product_of(n))
+    core_to_x(0)
+    to_core.append(product_of(3))
     for n in range(1, 4):
-        to_core.append(product_of(n))
-        core_to_x(n - 1)
-    core_to_x(3)
-
-    with jax.named_scope("w_bg_far"):
-        m_far.wait_recv()
-    m_near = stage("mn", [(mb.at[y, :, q], mb.at[y, :, q], at_z(d)) for d in (14, 1, 15)], mb.at[0, pl.ds(0, 3)])
-
-    near = []
+        core_to_x(n)
+
     for n in range(4):
         with jax.named_scope(f"w_x{n}"):
             to_x[n].wait_recv()
@@ -198,9 +194,9 @@
             remote(tsend.at[n], arecv.at[n], send_sem["a"], recv_sem["a"], at_z(order[n])).start()
     near = remote(arecv, arecv, send_sem["a"], recv_sem["a"], partner)
 
-    with jax.named_scope("w_bg_near"):
-        m_near.wait_recv()
-    m_tp = stage("my", [(mb.at[y], mb.at[y], at_y(d)) for d in (2, 1, 3)], mb.at[pl.ds(0, 3)])
+    with jax.named_scope("w_bg_far"):
+        m_far.wait_recv()
+    m_near = stage("mn", [(mb.at[y, :, q], mb.at[y, :, q], at_z(d)) for d in (14, 1, 15)], mb.at[0, pl.ds(0, 3)])
 
     with jax.named_scope("w_a"):
         near.wait_recv()
@@ -208,8 +204,13 @@
         total = total + arecv[n].astype(f32)
     brecv[k] = total.astype(bf16)
     far = stage("b", [(brecv.at[k], brecv.at[k], at_z(d)) for d in (8, 4, 12)], brecv.at[pl.ds(0, 3)])
+    with jax.named_scope("w_bg_near"):
+        m_near.wait_recv()
+    m_tp = stage("my", [(mb.at[y], mb.at[y], at_y(d)) for d in (2, 1, 3)], mb.at[pl.ds(0, 3)])
+
     with jax.named_scope("w_bg_wf"):
         w_far.wait_recv()
+    w_near = stage("wn", [(wb.at[:, q], wb.at[:, q], at_z(d)) for d in (14, 1, 15)], wb.at[pl.ds(0, 3)])
     with jax.named_scope("w_b"):
         far.wait_recv()
     total = brecv[0].astype(f32)
@@ -229,34 +230,25 @@
         key=lambda d: -(min(d[0], NZ - d[0]) + min(d[1], NX - d[1]) + min(d[3], NY - d[3]) + d[2] * 0.5),
     )[:-1]
 
-    def to_tp(part):
-        return [(gy.at[y, part], gy.at[y, part], at_y(d)) for d in (2, 1, 3)]
-
-    def start_tp(part):
-        for src, dst, to in to_tp(part):
-            remote(src, dst, send_sem["h"], recv_sem["h"], to).start()
-
-    spread = [remote(gy.at[y, q], gy.at[y, q], send_sem["g"], g_r.at[n], at_z(d)) for n, d in enumerate((14, 1, 15))]
-    for copy in spread:
-        copy.start()
-    start_tp(q)
+    def start_squares(some):
+        for dz, dx, dc, dy in some:
+            to = (zp(dz), xp(dx), c if dc == 0 else other, yp(dy))
+            remote(mine, mine, send_sem["sq"], recv_sem["sq"], to).start()
+
+    start_squares(around)
+    part = gy.at[y, q]
+    for dz in (14, 1, 15, 0):
+        for dy in (2, 1, 3):
+            remote(part, part, send_sem["h"], recv_sem["h"], (zp(dz), x, c, yp(dy))).start()
+    spread = stage("g", [(part, part, at_z(d)) for d in (14, 1, 15)], arecv)
     across = remote(gy.at[pl.ds(0, 3)], gy.at[pl.ds(0, 3)], send_sem["h"], recv_sem["h"], partner)
-    squares = stage(
-        "sq",
-        [(mine, mine, (zp(dz), xp(dx), c if dc == 0 else other, yp(dy))) for dz, dx, dc, dy in around],
-        sb.at[pl.ds(0, len(around))],
-    )
-    for n, d in ((1, 15), (2, 1)):
-        with jax.named_scope(f"w_c{n}"):
-            spread[n].wait_recv()
-        start_tp(lax.rem(zp(d), 4))
-    with jax.named_scope("w_c0"):
-        spread[0].wait_recv()
-    start_tp(lax.rem(zp(2), 4))
-    w_near = stage("wn", [(wb.at[:, q], wb.at[:, q], at_z(d)) for d in (14, 1, 15)], wb.at[pl.ds(0, 3)])
+    every = sb.at[pl.ds(0, len(around))]
+    squares = remote(every, every, send_sem["sq"], recv_sem["sq"], partner)
 
     with jax.named_scope("w_bg_y"):
         m_tp.wait_recv()
+    with jax.named_scope("w_c"):
+        spread.wait_recv()
     with jax.named_scope("w_y"):
         across.wait_recv()
     with jax.named_scope("w_s"):
@@ -290,41 +282,47 @@
     def to_partner(part, which):
         send_piece(part, which, o_s.at[12], o_r.at[12], partner)
 
-    for part in (0, 3, 1, 2):
-        pieces = []
-        for t in range(NY):
-            scaled = clip_factor * gy[t, part].astype(f32)
-            first_new = beta_first * mb[t, part, :, 0].reshape(32, 128) + (1.0 - beta_first) * scaled
-            second_new = beta_second * mb[t, part, :, 1].reshape(32, 128) + (1.0 - beta_second) * scaled * scaled
-            firsts[t, pl.ds(part * 4, 4)] = first_new.reshape(4, 8, 128)
-            seconds[t, pl.ds(part * 4, 4)] = second_new.reshape(4, 8, 128)
-            pieces.append(first_new / (jnp.sqrt(second_new) + small_eps))
-        direction = jnp.concatenate(pieces, axis=1)
+    for batch in ((0, 3), (1, 2)):
+        rows = []
+        for part in batch:
+            pieces = []
+            for t in range(NY):
+                scaled = clip_factor * gy[t, part].astype(f32)
+                first_new = beta_first * mb[t, part, :, 0].reshape(32, 128) + (1.0 - beta_first) * scaled
+                second_new = beta_second * mb[t, part, :, 1].reshape(32, 128) + (1.0 - beta_second) * scaled * scaled
+                firsts[t, pl.ds(part * 4, 4)] = first_new.reshape(4, 8, 128)
+                seconds[t, pl.ds(part * 4, 4)] = second_new.reshape(4, 8, 128)
+                pieces.append(first_new / (jnp.sqrt(second_new) + small_eps))
+            rows.append(jnp.concatenate(pieces, axis=1))
+        direction = jnp.concatenate(rows, axis=0)
         upper = direction.astype(bf16)
         lower = (direction - upper.astype(f32)).astype(bf16)
-        product = lax.dot_general(
-            jnp.concatenate([upper, lower], axis=0), wt[...], (((1,), (1,)), ((), ())), preferred_element_type=f32
-        )
-        product = product[0:32] + product[32:64]
-        upd[pl.ds(part * 4, 4)] = product.reshape(4, 8, 2 * NW)
-        if part == 0:
+        product = jnp.dot(jnp.concatenate([upper, lower], axis=0), wtt[...], preferred_element_type=f32)
+        product = product[0:64] + product[64:128]
+        if batch[0] == 0:
             with jax.named_scope("w_bg_wn"):
                 w_near.wait_recv()
-        old = wb[part].astype(f32)
-        moved = jnp.stack(
-            [product[:, 0:NW].reshape(4, 8, NW), product[:, NW : 2 * NW].reshape(4, 8, NW)], axis=1
-        ).reshape(4, 16, NW)
-        new = (old - step_rate * moved).astype(bf16)
-        ko_ref[pl.ds(part * 4, 4), xc] = new[:, :, 0:NK]
-        vo_ref[pl.ds(part * 4, 4), xc] = new[:, :, NK:NW]
-        if part != 3:
-            to_right(part, xc)
-        if part >= 2:
-            to_left(part, xc)
-        to_partner(part, xc)
-    to_left(1, xc)
-    to_right(3, xc)
-    to_left(0, xc)
+        for n, part in enumerate(batch):
+            change = product[n * 32 : n * 32 + 32]
+            upd[pl.ds(part * 4, 4)] = change.reshape(4, 8, 2 * NW)
+            moved = jnp.stack(
+                [change[:, 0:NW].reshape(4, 8, NW), change[:, NW : 2 * NW].reshape(4, 8, NW)], axis=1
+            ).reshape(4, 16, NW)
+            new = (wb[part].astype(f32) - step_rate * moved).astype(bf16)
+            ko_ref[pl.ds(part * 4, 4), xc] = new[:, :, 0:NK]
+            vo_ref[pl.ds(part * 4, 4), xc] = new[:, :, NK:NW]
+        if batch[0] == 0:
+            to_right(0, xc)
+            to_left(3, xc)
+        else:
+            to_right(1, xc)
+            to_left(2, xc)
+            to_right(2, xc)
+            to_left(1, xc)
+            to_right(3, xc)
+            to_left(0, xc)
+        for part in batch:
+            to_partner(part, xc)
 
     for out, packed_all in ((first_ref, firsts), (second_ref, seconds)):
         packed = packed_all[y, z]
@@ -339,11 +337,9 @@
         nk_ref[rows, :] = kvw[rows, 0:NK] - step_rate * own_upd[:, at : at + NK]
         nv_ref[rows, :] = kvw[rows, NK:NW] - step_rate * own_upd[:, at + NK : at + NW]
 
-    finish.append(near)
-    finish.append(across)
+    finish.extend([near, across, squares])
     for copy in to_core + to_x + finish:
         copy.wait_send()
-    remote(arecv, arecv, send_sem["g"], g_r.at[0], partner).wait_send()
 
     for n in range(6):
         with jax.named_scope(f"w_r{n}"):
@@ -395,12 +391,12 @@
         out_specs=[vmem] * 6,
         scratch_shapes=[
             pltpu.VMEM((TOK, D), bf16),
-            pltpu.VMEM((D, TOK), bf16),
             pltpu.VMEM((TOK, NW), bf16),
             pltpu.VMEM((NW, RANK), bf16),
             pltpu.VMEM((16, NW), f32),
             pltpu.VMEM((2, 2, 16, 32), f32),
             pltpu.VMEM((2 * NW, 4 * 128), bf16),
+            pltpu.VMEM((4 * 128, 2 * NW), bf16),
             pltpu.VMEM((NY, HALF, 128), bf16),
             pltpu.VMEM((NY - 1, HALF, 128), bf16),
             pltpu.VMEM((4, NX, NC, 32, 128), bf16),
@@ -417,7 +413,7 @@
             pltpu.VMEM((NY, 16, 8, 128), f32),
             pltpu.VMEM((NY, 16, 8, 128), f32),
             pltpu.VMEM((16, 8, 2 * NW), f32),
-            dma((5,)), dma((4,)), dma((4,)), dma((4,)), dma((4,)), dma((3,)), dma((13,)), dma((13,)), dma((11,)), dma((11,)),
+            dma((5,)), dma((4,)), dma((4,)), dma((4,)), dma((4,)), dma((13,)), dma((13,)), dma((11,)), dma((11,)),
         ],
         compiler_params=pltpu.CompilerParams(
             collective_id=0, has_side_effects=True, vmem_limit_bytes=40 * 1024 * 1024

time: 57.8 us -> 56.5 us (0.978)
  Pallas kernels: 57 us -> 55.7 us
    pallas_call x1, Pallas kernels: 55.8 us -> 54.5 us  [local(): pl.pallas_call(kernel, out_shape=(shape((2, 16, 32), f32), shape((2, 16,...]
where the time goes in v5:
time: 56.5 us; the launch traced here: 56.4 us
  Pallas kernels  55.7 us (99%)
  between operations  0.64 us (1%)
    pallas_call x1, Pallas kernels, local(): pl.pallas_call(kernel, out_shape=(shape((2, 16, 32), f32), shape((2, 16,...  54.5 us
    pallas_call x1, Pallas kernels, local(): pl.pallas_call(store, out_shape=tuple((shape(r.shape, r.dtype) for r in r...  1.2 us

profile of v5, /device:TPU:1, one launch (start us, length us, event | category | flops | bytes accessed | tf_op | source)
XLA Modules:
  0.0 56.4 jit_solution(2060182246897070809)
XLA Ops:
  0.6 54.5 %step.1 = (f32[2,16,32]{2,1,0:T(8,128)S(1)}, f32[2,16,32]{2,1,0:T(8,128)S(1)}, f32[16,128]{1,0:T(8,128)S(1)}, f32[16,256]{1,0:T(8,128)S(1)}, bf16[16,8,16,128]{3...) custom-call(bf16[640,2048]{1,0:T(8,128)(2,1)} %x_hbm.1, bf16[640,128]{1,0:T(8,128)(2,1)} %ck_hbm.1, ...), custom_call_target="tpu_custom_call" | custom-call | tf_op jit(solution)/shard_map/step/pallas_call | solution.py:380
  55.2 1.2 %store.1 = (f32[2,16,32]{2,1,0:T(8,128)}, f32[2,16,32]{2,1,0:T(8,128)}, f32[16,128]{1,0:T(8,128)}, f32[16,256]{1,0:T(8,128)}, bf16[2048,128]{1,0:T(8,128)(2,1)}, /*index=5*/bf16[2048,256]{1,0:T(8,128)(2,1)}) custom-call(f32[2,16,32]{2,1,0:T(8,128)S(1)} %get-tuple-element.12.refs_0_, f32[2,16,32]{2,1,0:T(8,128)S(1)} %get-tuple-element.13.refs_1_, ...), custom_call_target="tpu_custom_call" | custom-call | tf_op jit(solution)/shard_map/store/pallas_call | solution.py:424

commit v6 on v5

--- a/solution.py
+++ b/solution.py
@@ -33,7 +33,7 @@
     first_ref, second_ref, nk_ref, nv_ref, ko_ref, vo_ref,
     x_vm, ckv, fkv, kvw, mv, wt, wtt, msend, yrecv, asend, crecv, xsend, xrecv, tsend, arecv, brecv, gy, mb, wb, sb,
     firsts, seconds, upd,
-    in_sem, c_s, c_r, x_s, x_r, o_s, o_r, one_s, one_r,
+    in_sem, ahead, c_s, c_r, x_s, x_r, o_s, o_r, one_s, one_r,
 ):
     z, x, c, y = (lax.axis_index(n) for n in ("z", "x", "c", "y"))
     k, q = lax.div(z, 4), lax.rem(z, 4)
@@ -91,7 +91,7 @@
 
     for load in load_f + load_c:
         load.start()
-    sources = [at_z(d) for d in FAR + (2, 15, 1)] + [at_y(d) for d in (2, 1, 3)] + [at_x(d) for d in (2, 1, 3)] + [partner]
+    sources = [at_z(d) for d in (2, 14, 15, 1)] + [at_y(d) for d in (2, 1, 3)] + [at_x(d) for d in (2, 1, 3)] + [partner]
     barrier = pltpu.get_barrier_semaphore()
     for peer in sources:
         pl.semaphore_signal(barrier, inc=1, device_id=peer, device_id_type=pl.DeviceIdType.MESH)
@@ -130,12 +130,34 @@
         pl.semaphore_wait(barrier, len(sources))
 
     tp = stage("tp", [(msend.at[yp(d)], yrecv.at[d - 1], at_y(d)) for d in (2, 1, 3)], yrecv)
-    m_far = stage("mf", [(mb.at[y, k, q], mb.at[y, k, q], at_z(d)) for d in (8, 4, 12)], mb.at[0, 0, pl.ds(0, 3)])
-    w_far = stage("wf", [(wb.at[k, q], wb.at[k, q], at_z(d)) for d in (8, 4, 12)], wb.at[0, pl.ds(0, 3)])
+
+    def signal(n, to):
+        pl.semaphore_signal(ahead.at[n], inc=1, device_id=to, device_id_type=pl.DeviceIdType.MESH)
+
+    signal(0, at_z(2))
+    signal(0, at_z(14))
 
     load_x.wait()
     for n in range(4):
         wtt[pl.ds(n * 128, 128), :] = wt[:, n * 128 : (n + 1) * 128].T
+
+    def start_far(d):
+        remote(mb.at[y, k, q], mb.at[y, k, q], send_sem["mf"], recv_sem["mf"], at_z(d)).start()
+        remote(wb.at[k, q], wb.at[k, q], send_sem["wf"], recv_sem["wf"], at_z(d)).start()
+
+    with jax.named_scope("w_f1"):
+        pl.semaphore_wait(ahead.at[0], 2)
+    signal(1, at_z(4))
+    signal(1, at_z(12))
+    start_far(4)
+    start_far(12)
+    with jax.named_scope("w_f2"):
+        pl.semaphore_wait(ahead.at[1], 2)
+    start_far(8)
+    three = mb.at[0, 0, pl.ds(0, 3)]
+    m_far = remote(three, three, send_sem["mf"], recv_sem["mf"], partner)
+    three = wb.at[0, pl.ds(0, 3)]
+    w_far = remote(three, three, send_sem["wf"], recv_sem["wf"], partner)
 
     with jax.named_scope("w_tp"):
         tp.wait_recv()
@@ -194,16 +216,16 @@
             remote(tsend.at[n], arecv.at[n], send_sem["a"], recv_sem["a"], at_z(order[n])).start()
     near = remote(arecv, arecv, send_sem["a"], recv_sem["a"], partner)
 
-    with jax.named_scope("w_bg_far"):
-        m_far.wait_recv()
-    m_near = stage("mn", [(mb.at[y, :, q], mb.at[y, :, q], at_z(d)) for d in (14, 1, 15)], mb.at[0, pl.ds(0, 3)])
-
     with jax.named_scope("w_a"):
         near.wait_recv()
     for n in range(3):
         total = total + arecv[n].astype(f32)
     brecv[k] = total.astype(bf16)
     far = stage("b", [(brecv.at[k], brecv.at[k], at_z(d)) for d in (8, 4, 12)], brecv.at[pl.ds(0, 3)])
+    with jax.named_scope("w_bg_far"):
+        m_far.wait_recv()
+    m_near = stage("mn", [(mb.at[y, :, q], mb.at[y, :, q], at_z(d)) for d in (14, 1, 15)], mb.at[0, pl.ds(0, 3)])
+
     with jax.named_scope("w_bg_near"):
         m_near.wait_recv()
     m_tp = stage("my", [(mb.at[y], mb.at[y], at_y(d)) for d in (2, 1, 3)], mb.at[pl.ds(0, 3)])
@@ -337,7 +359,7 @@
         nk_ref[rows, :] = kvw[rows, 0:NK] - step_rate * own_upd[:, at : at + NK]
         nv_ref[rows, :] = kvw[rows, NK:NW] - step_rate * own_upd[:, at + NK : at + NW]
 
-    finish.extend([near, across, squares])
+    finish.extend([near, across, squares, m_far, w_far])
     for copy in to_core + to_x + finish:
         copy.wait_send()
 
@@ -413,7 +435,7 @@
             pltpu.VMEM((NY, 16, 8, 128), f32),
             pltpu.VMEM((NY, 16, 8, 128), f32),
             pltpu.VMEM((16, 8, 2 * NW), f32),
-            dma((5,)), dma((4,)), dma((4,)), dma((4,)), dma((4,)), dma((13,)), dma((13,)), dma((11,)), dma((11,)),
+            dma((5,)), pltpu.SemaphoreType.REGULAR((2,)), dma((4,)), dma((4,)), dma((4,)), dma((4,)), dma((13,)), dma((13,)), dma((11,)), dma((11,)),
         ],
         compiler_params=pltpu.CompilerParams(
             collective_id=0, has_side_effects=True, vmem_limit_bytes=40 * 1024 * 1024

time: 56.5 us -> 54.9 us (0.972)
  Pallas kernels: 55.7 us -> 54.1 us
    pallas_call x1, Pallas kernels: 54.5 us -> 52.9 us  [local(): pl.pallas_call(kernel, out_shape=(shape((2, 16, 32), f32), shape((2, 16,...]
where the time goes in v6:
time: 54.9 us; the launch traced here: 54.8 us
  Pallas kernels  54.1 us (99%)
  between operations  0.64 us (1%)
    pallas_call x1, Pallas kernels, local(): pl.pallas_call(kernel, out_shape=(shape((2, 16, 32), f32), shape((2, 16,...  52.9 us
    pallas_call x1, Pallas kernels, local(): pl.pallas_call(store, out_shape=tuple((shape(r.shape, r.dtype) for r in r...  1.2 us

profile of v6, /device:TPU:1, one launch (start us, length us, event | category | flops | bytes accessed | tf_op | source)
XLA Modules:
  0.0 54.8 jit_solution(14033889233134216560)
XLA Ops:
  0.6 52.9 %step.1 = (f32[2,16,32]{2,1,0:T(8,128)S(1)}, f32[2,16,32]{2,1,0:T(8,128)S(1)}, f32[16,128]{1,0:T(8,128)S(1)}, f32[16,256]{1,0:T(8,128)S(1)}, bf16[16,8,16,128]{3...) custom-call(bf16[640,2048]{1,0:T(8,128)(2,1)} %x_hbm.1, bf16[640,128]{1,0:T(8,128)(2,1)} %ck_hbm.1, ...), custom_call_target="tpu_custom_call" | custom-call | tf_op jit(solution)/shard_map/step/pallas_call | solution.py:402
  53.6 1.2 %store.1 = (f32[2,16,32]{2,1,0:T(8,128)}, f32[2,16,32]{2,1,0:T(8,128)}, f32[16,128]{1,0:T(8,128)}, f32[16,256]{1,0:T(8,128)}, bf16[2048,128]{1,0:T(8,128)(2,1)}, /*index=5*/bf16[2048,256]{1,0:T(8,128)(2,1)}) custom-call(f32[2,16,32]{2,1,0:T(8,128)S(1)} %get-tuple-element.12.refs_0_, f32[2,16,32]{2,1,0:T(8,128)S(1)} %get-tuple-element.13.refs_1_, ...), custom_call_target="tpu_custom_call" | custom-call | tf_op jit(solution)/shard_map/store/pallas_call | solution.py:446
